TPU v7x, 32 devices: a whole 2x2x4 slice. The times are simulated.
32 devices in a mesh: sp: 8 (over z, x), tp: 4 (over y, core).
Axes of the slice: x: 2, y: 2, z: 4, core: 2. Of those that a mesh axis runs over, the one named last changes fastest.
Arguments:
- cotangent: bfloat16 [1024, 2048], P('sp'), may hold values from -6 to 6
- mixer_out: bfloat16 [1024, 2048], P('sp'), may hold values from -6 to 6
- expert_ids: int32 [1024, 2], P('sp'), may hold values from 0 to 7, all different within a row; in each aligned block of 128 rows (0 to 127, 128 to 255, ...) at most 64 rows name the same one
- route_weight: float32 [1024, 2], P('sp'), may hold values from 0.3 to 1.5
- saved_normalized: bfloat16 [1024, 2048], P('sp', 'tp'), may hold values from -6 to 6
- inverse_deviation: float32 [1024], P('sp'), may hold values from 0.3 to 3
- channel_norm_gain: float32 [2048], P('tp'), may hold values from 0.1 to 1.9
- taps: float32 [31, 2048], P(None, 'tp'), may hold values from -1 to 1
- proj_weight: bfloat16 [2048, 2048], P('tp'), may hold values from -0.125 to 0.125
- gate_weight: bfloat16 [8, 2048, 2048], P('sp', None, 'tp'), may hold values from -0.125 to 0.125
- up_weight: bfloat16 [8, 2048, 2048], P('sp', None, 'tp'), may hold values from -0.125 to 0.125
- down_weight: bfloat16 [8, 2048, 2048], P('sp', 'tp'), may hold values from -0.125 to 0.125
Outputs:
- grad_mixer_in: bfloat16 [1024, 2048], P('sp', 'tp')
- grad_proj: float32 [2048, 2048], P('sp', 'tp')
- grad_gate: bfloat16 [8, 2048, 2048], P('sp', None, 'tp')
- grad_up: bfloat16 [8, 2048, 2048], P('sp', None, 'tp')
- grad_down: bfloat16 [8, 2048, 2048], P('sp', 'tp')
Inputs may be any that keep to these rules, and one draw needn't show every extreme that they name: `expert_ids`: each row names 2 different experts. Within the rows of one index of sp no expert is named more than 64 times, a bound that some block reaches.
All inputs are finite; a program needn't handle non-finite values.
Results may differ from a plain program's by a relative error of at most 0.02.
Values may be sent and summed in bfloat16 or wider, within the bound.
A program may use at most 64 MiB of HBM per device.

v0:
```python
import jax
import jax.numpy as jnp
from jax import lax
from jax.sharding import PartitionSpec as P


def from_behind(value, axis, steps):
    count = lax.axis_size(axis)
    leading, last = (max(0, -steps), min(count, count - steps))
    return lax.ppermute(value, axis, [(source, source + steps) for source in range(leading, last)])


def route_table(expert_ids, route_weight, slot_start, slot_span, capacity, experts):
    onehot = (expert_ids[:, :, None] == jnp.arange(experts, dtype=jnp.int32)[None, None, :]).astype(
        jnp.int32
    )
    flat_hot = onehot.reshape(-1, experts)
    ranks = jnp.cumsum(flat_hot, axis=0) - flat_hot
    rank_pair = jnp.sum(ranks * flat_hot, axis=1).reshape(expert_ids.shape)
    slot_index = expert_ids * capacity + rank_pair
    targets = (
        jnp.arange(experts, dtype=jnp.int32)[:, None] * capacity
        + slot_start
        + jnp.arange(slot_span, dtype=jnp.int32)[None, :]
    ).reshape(-1)
    matched = slot_index[None, :, :] == targets[:, None, None]
    dispatch = jnp.any(matched, axis=2).astype(jnp.bfloat16)
    slot_weight = jnp.sum(jnp.where(matched, route_weight[None, :, :], 0.0), axis=(1, 2))
    return (dispatch, slot_weight)


def shards(
    cotangent,
    mixer_out,
    expert_ids,
    route_weight,
    saved_normalized,
    inverse_deviation,
    channel_norm_gain,
    taps,
    proj_weight,
    gate_weight,
    up_weight,
    down_weight,
):
    experts = lax.axis_size("sp")
    groups = lax.axis_size("tp")
    tok_rows, model_width = cotangent.shape
    capacity = groups * max(1, 4 * tok_rows // (experts * groups))
    slot_span = capacity // groups
    slot_start = lax.axis_index("tp") * slot_span
    dispatch, slot_weight = route_table(
        expert_ids, route_weight, slot_start, slot_span, capacity, experts
    )
    sent_rows = jnp.dot(dispatch, mixer_out, preferred_element_type=jnp.float32).astype(
        jnp.bfloat16
    )
    sent_grad = (
        slot_weight[:, None] * jnp.dot(dispatch, cotangent, preferred_element_type=jnp.float32)
    ).astype(jnp.bfloat16)
    sent_rows = sent_rows.reshape(experts, slot_span, model_width)
    sent_grad = sent_grad.reshape(experts, slot_span, model_width)
    shared_rows = (
        lax.all_to_all(sent_rows, "sp", split_axis=0, concat_axis=0, tiled=True),
        lax.all_to_all(sent_grad, "sp", split_axis=0, concat_axis=0, tiled=True),
    )
    routed_rows, routed_grad = (
        lax.all_gather(shared_rows[0], "tp", axis=1, tiled=True),
        lax.all_gather(shared_rows[1], "tp", axis=1, tiled=True),
    )
    full_table, unused_weight = route_table(
        expert_ids, route_weight, 0, capacity, capacity, experts
    )
    routed_rows = routed_rows.reshape(-1, model_width)
    routed_grad = routed_grad.reshape(-1, model_width)
    w_first = gate_weight[0]
    w_third = up_weight[0]
    w_second = down_weight[0]
    contract_last = (((1,), (1,)), ((), ()))
    contract_first = (((0,), (0,)), ((), ()))
    hidden_gate = jnp.dot(routed_rows, w_first, preferred_element_type=jnp.float32)
    hidden_up = jnp.dot(routed_rows, w_third, preferred_element_type=jnp.float32)
    sigma = jax.nn.sigmoid(hidden_gate)
    swish = hidden_gate * sigma
    activ = (swish * hidden_up).astype(jnp.bfloat16)
    grad_second = lax.dot_general(
        activ, routed_grad, contract_first, preferred_element_type=jnp.float32
    ).astype(jnp.bfloat16)
    grad_activ = lax.dot_general(
        routed_grad, w_second, contract_last, preferred_element_type=jnp.float32
    )
    grad_gpre = (grad_activ * hidden_up * sigma * (1.0 + hidden_gate * (1.0 - sigma))).astype(
        jnp.bfloat16
    )
    grad_upre = (grad_activ * swish).astype(jnp.bfloat16)
    grad_first = lax.dot_general(
        routed_rows, grad_gpre, contract_first, preferred_element_type=jnp.float32
    ).astype(jnp.bfloat16)
    grad_third = lax.dot_general(
        routed_rows, grad_upre, contract_first, preferred_element_type=jnp.float32
    ).astype(jnp.bfloat16)
    partial_value = lax.dot_general(
        grad_gpre, w_first, contract_last, preferred_element_type=jnp.float32
    ) + lax.dot_general(grad_upre, w_third, contract_last, preferred_element_type=jnp.float32)
    summed = lax.psum(partial_value.astype(jnp.bfloat16), "tp")
    home_rows = lax.all_to_all(
        summed.reshape(experts, capacity, model_width),
        "sp",
        split_axis=0,
        concat_axis=0,
        tiled=True,
    )
    returned = lax.dot_general(
        full_table,
        home_rows.reshape(-1, model_width),
        contract_first,
        preferred_element_type=jnp.float32,
    )
    mixer_grad = (cotangent.astype(jnp.float32) + returned).astype(jnp.bfloat16)
    normalized_input = saved_normalized.astype(jnp.float32)
    normalized_values = normalized_input * channel_norm_gain[None, :]
    gate_sig = jax.nn.sigmoid(normalized_values)
    act_conv = (normalized_values * gate_sig).astype(jnp.bfloat16)
    grad_proj = lax.psum_scatter(
        lax.dot_general(
            mixer_grad, act_conv, contract_first, preferred_element_type=jnp.float32
        ).astype(jnp.bfloat16),
        "sp",
        scatter_dimension=0,
        tiled=True,
    ).astype(jnp.float32)
    grad_act = lax.dot_general(
        mixer_grad, proj_weight, contract_last, preferred_element_type=jnp.float32
    )
    norm_output_gradient = (
        grad_act
        * gate_sig
        * (1.0 + normalized_values * (1.0 - gate_sig))
        * channel_norm_gain[None, :]
    )
    reduced_totals = lax.psum(
        (
            jnp.sum(norm_output_gradient, axis=1),
            jnp.sum(norm_output_gradient * normalized_input, axis=1),
        ),
        "tp",
    )
    channel_count = saved_normalized.shape[1] * groups
    conv_output_gradient = inverse_deviation[:, None] * (
        norm_output_gradient
        - reduced_totals[0][:, None] / channel_count
        - normalized_input * (reduced_totals[1][:, None] / channel_count)
    )
    reach = taps.shape[0] - 1
    beyond = from_behind(conv_output_gradient[:reach], "sp", -1)
    extended = jnp.concatenate([conv_output_gradient, beyond], axis=0)
    result = jnp.zeros_like(conv_output_gradient)
    for tap_index in range(taps.shape[0]):
        result = result + taps[tap_index][None, :] * extended[tap_index : tap_index + tok_rows]
    return (
        result.astype(jnp.bfloat16),
        grad_proj,
        grad_first[None],
        grad_third[None],
        grad_second[None],
    )


def solution(mesh):
    return jax.shard_map(
        shards,
        mesh=mesh,
        in_specs=(
            P("sp", None),
            P("sp", None),
            P("sp", None),
            P("sp", None),
            P("sp", "tp"),
            P("sp"),
            P("tp"),
            P(None, "tp"),
            P("tp", None),
            P("sp", None, "tp"),
            P("sp", None, "tp"),
            P("sp", "tp", None),
        ),
        out_specs=(
            P("sp", "tp"),
            P("sp", "tp"),
            P("sp", None, "tp"),
            P("sp", None, "tp"),
            P("sp", "tp", None),
        ),
        check_vma=False,
    )
```

profile of v0, /device:TPU:0, one launch (start us, length us, event | category | flops | bytes accessed | tf_op | source)
XLA Modules:
  0.0 273.1 jit_solution(8081440627756328696)
XLA Ops:
  7.3 0.9 copy.31
  8.6 0.6 reduce-window.6
  9.8 0.7 multiply_add_fusion
  10.6 1.3 convolution_convert_fusion.4
  11.9 21.7 %all_to_all.15 = bf16[8,16,2048]{2,1,0:T(8,128)(2,1)} all-to-all(bf16[8,16,2048]{2,1,0:T(8,128)(2,1)S(1)} %bitcast.87), channel_id=1, replica_groups=mesh['sp'=8,'tp'=4] {'sp'}, dimensions={0} | all-to-all | bytes 1048576 | tf_op jit(solution)/shard_map/all_to_all | solution.py:64
  34.2 17.6 %all_to_all.16 = bf16[8,16,2048]{2,1,0:T(8,128)(2,1)} all-to-all(bf16[8,16,2048]{2,1,0:T(8,128)(2,1)S(1)} %bitcast.86), channel_id=1, replica_groups=mesh['sp'=8,'tp'=4] {'sp'}, dimensions={0} | all-to-all | bytes 1048576 | tf_op jit(solution)/shard_map/all_to_all | solution.py:65
  51.9 3.5 %all-gather.5.cloned.1.call-done = bf16[8,64,2048]{2,1,0:T(8,128)(2,1)} async-done(((bf16[8,16,2048]{2,1,0:T(8,128)(2,1)}), bf16[8,64,2048]{2,1,0:T(8,128)(2,1)}) %all-gather.5.cloned.1.call-update) | async-done | bytes 2097168 | tf_op jit(solution)/shard_map/all_gather | solution.py:68
  55.4 4.0 %fusion.7 = f32[512,512]{1,0:T(8,128)} fusion(bf16[512,2048]{1,0:T(8,128)(2,1)} %bitcast.119, bf16[1,2048,512]{2,1,0:T(8,128)(2,1)S(1)} %copy-done), kind=kOutput, calls=%fused_computation.44 | convolution fusion | flops 1073741824 | bytes 5242880 | tf_op jit(solution)/shard_map/dot_general | solution.py:81
  59.4 2.3 fusion.10
  61.7 17.9 %all-gather.3.cloned.1.call-done = bf16[8,64,2048]{2,1,0:T(8,128)(2,1)} async-done(((bf16[8,16,2048]{2,1,0:T(8,128)(2,1)}), bf16[8,64,2048]{2,1,0:T(8,128)(2,1)}) %all-gather.3.cloned.1.call-update) | async-done | bytes 2097168 | tf_op jit(solution)/shard_map/all_gather | solution.py:69
  79.6 4.4 %multiply_convert_fusion.1 = (bf16[512,512]{1,0:T(8,128)(2,1)S(1)}, bf16[512,512]{1,0:T(8,128)(2,1)S(1)}) fusion(f32[512,512]{1,0:T(8,128)} %fusion.7, f32[512,512]{1,0:T(8,128)} %fusion.10, bf16[512,2048]{1,0:T(8,128)(2,1)} %bitcast.123, bf16[1,512,2048]{2,1,0:T(8,128)(2,1)} %param.23), kind=kOutput, calls=%fused_computation.55 | convolution fusion | flops 1077149696 | bytes 7340032 | tf_op jit(solution)/shard_map/dot_general | solution.py:89
  84.0 1.3 fusion.5
  85.3 0.6 copy-done.2
  85.9 2.6 add_convert_fusion
  88.6 51.5 %all-reduce.3.cloned.1.call-done = bf16[8,64,2048]{2,1,0:T(8,128)(2,1)} async-done(((bf16[8,64,2048]{2,1,0:T(8,128)(2,1)}), bf16[8,64,2048]{2,1,0:T(8,128)(2,1)}) %all-reduce.3.cloned.1.call-update) | async-done | bytes 2097168 | tf_op jit(solution)/shard_map/psum | solution.py:105
  140.1 5.5 %all-to-all-start.2 = ((bf16[8,64,2048]{2,1,0:T(8,128)(2,1)}), bf16[8,64,2048]{2,1,0:T(8,128)(2,1)}, u32[]{:S(2)}, u32[]{:S(2)}) async-start(bf16[8,64,2048]{2,1,0:T(8,128)(2,1)} %all-reduce.3.cloned.1.call-done), calls=%async_computation.2 | async-start | bytes 4194304 | tf_op jit(solution)/shard_map/all_to_all | solution.py:106
  146.0 47.7 %all-to-all-done.2 = bf16[8,64,2048]{2,1,0:T(8,128)(2,1)} async-done(((bf16[8,64,2048]{2,1,0:T(8,128)(2,1)}), bf16[8,64,2048]{2,1,0:T(8,128)(2,1)}, u32[]{:S(2)}, u32[]{:S(2)}) %all-to-all-start.2) | async-done | bytes 2097184 | tf_op jit(solution)/shard_map/all_to_all | solution.py:106
  193.7 2.1 fusion.4
  195.8 2.1 convolution_convert_fusion
  198.0 0.6 fusion.130
  198.6 0.7 fusion.129
  199.3 4.4 %fusion.1 = bf16[1,2048,512]{2,1,0:T(8,128)(2,1)} fusion(bf16[512,2048]{1,0:T(8,128)(2,1)} %bitcast.120, bf16[512,512]{1,0:T(8,128)(2,1)S(1)} %copy-done.7), kind=kOutput, calls=%fused_computation.35 | convolution fusion | flops 1074790400 | bytes 4718592 | tf_op jit(solution)/shard_map/dot_general | solution.py:99
  203.7 2.7 fusion.2
  206.4 1.5 fusion.128
  207.9 6.2 %all-reduce = (f32[128]{0:T(128)S(1)}, f32[128]{0:T(128)S(1)}) all-reduce(f32[128]{0:T(128)} %get-tuple-element.6, f32[128]{0:T(128)} %get-tuple-element.5), channel_id=1, replica_groups=mesh['sp'=8,'tp'=4] {'tp'}, use_global_device_ids=true, to_apply=%region_10.11 | all-reduce | flops 256 | bytes 2048 | tf_op jit(solution)/shard_map/psum | solution.py:141
  214.1 0.8 fusion.27
  215.2 1.3 collective-permute-start
  216.5 4.3 %fusion = bf16[1,2048,512]{2,1,0:T(8,128)(2,1)} fusion(bf16[512,2048]{1,0:T(8,128)(2,1)} %bitcast.121, bf16[512,512]{1,0:T(8,128)(2,1)S(1)} %copy-done.5), kind=kOutput, calls=%fused_computation.34 | convolution fusion | flops 1074790400 | bytes 4718592 | tf_op jit(solution)/shard_map/dot_general | solution.py:96
  220.7 0.9 collective-permute-done
  221.9 2.0 fusion.32
  223.9 40.9 %reduce-scatter.2.cloned.1.call-done = bf16[256,512]{1,0:T(8,128)(2,1)} async-done(((bf16[2048,512]{1,0:T(8,128)(2,1)}), bf16[256,512]{1,0:T(8,128)(2,1)}) %reduce-scatter.2.cloned.1.call-update) | async-done | bytes 262160 | tf_op jit(solution)/shard_map/reduce_scatter | solution.py:124
  264.8 1.8 convert_element_type.72
  (118 shorter events, 2.3 us)
Async XLA Ops:
  7.2 48.3 %copy-start = (bf16[1,2048,512]{2,1,0:T(8,128)(2,1)S(1)}, bf16[1,2048,512]{2,1,0:T(8,128)(2,1)}, u32[]{:S(2)}) copy-start(bf16[1,2048,512]{2,1,0:T(8,128)(2,1)} %param.21) | copy-start | bytes 6291460
  7.2 26.5 %copy-start.39 = (f32[128,2]{0,1:T(2,128)S(1)}, f32[128,2]{0,1:T(2,128)}, u32[]{:S(2)}) copy-start(f32[128,2]{0,1:T(2,128)} %param.15) | copy-start | bytes 3076
  7.2 26.7 %copy-start.3 = (bf16[128,2048]{1,0:T(8,128)(2,1)S(1)}, bf16[128,2048]{1,0:T(8,128)(2,1)}, u32[]{:S(2)}) copy-start(bf16[128,2048]{1,0:T(8,128)(2,1)} %param.12) | copy-start | bytes 1572868
  7.2 48.2 %all-gather.5.cloned.1.call-start = ((), (), s32[]{:S(2)}) async-start(), calls=%async_computation.5 | async-start | bytes 2621440 | tf_op jit(solution)/shard_map/all_gather | solution.py:68
  33.7 45.9 %all-gather.3.cloned.1.call-start = ((), (), s32[]{:S(2)}) async-start(), calls=%async_computation.4 | async-start | bytes 2621440 | tf_op jit(solution)/shard_map/all_gather | solution.py:69
  51.9 88.2 %all-reduce.3.cloned.1.call-start = ((), (), s32[]{:S(2)}) async-start(), calls=%async_computation.6 | async-start | bytes 4194304 | tf_op jit(solution)/shard_map/psum | solution.py:105
  140.1 53.6 %all-to-all-start.2 = ((bf16[8,64,2048]{2,1,0:T(8,128)(2,1)}), bf16[8,64,2048]{2,1,0:T(8,128)(2,1)}, u32[]{:S(2)}, u32[]{:S(2)}) async-start(bf16[8,64,2048]{2,1,0:T(8,128)(2,1)} %all-reduce.3.cloned.1.call-done), calls=%async_computation.2 | async-start | bytes 4194304 | tf_op jit(solution)/shard_map/all_to_all | solution.py:106
  145.6 50.2 %copy-start.8 = (bf16[128,512]{1,0:T(8,128)(2,1)S(1)}, bf16[128,512]{1,0:T(8,128)(2,1)}, u32[]{:S(2)}) copy-start(bf16[128,512]{1,0:T(8,128)(2,1)} %param.16) | copy-start | bytes 393220
  145.6 50.2 %copy-start.37 = (f32[512]{0:T(512)S(1)}, f32[512]{0:T(512)}, u32[]{:S(2)}) copy-start(f32[512]{0:T(512)} %param.18) | copy-start | bytes 6148
  145.6 119.1 %reduce-scatter.2.cloned.1.call-start = ((), (), s32[]{:S(2)}) async-start(), calls=%async_computation.7 | async-start | bytes 2359296 | tf_op jit(solution)/shard_map/reduce_scatter | solution.py:124
  206.4 10.0 %copy-start.5 = (bf16[512,512]{1,0:T(8,128)(2,1)S(1)}, bf16[512,512]{1,0:T(8,128)(2,1)}, u32[]{:S(2)}) copy-start(bf16[512,512]{1,0:T(8,128)(2,1)} %copy-done.4) | copy-start | bytes 1572868
  214.9 6.8 %copy-start.10 = (f32[1,512]{1,0:T(1,128)S(1)}, f32[1,512]{1,0:T(1,128)}, u32[]{:S(2)}) copy-start(f32[1,512]{1,0:T(1,128)} %get-tuple-element.34) | copy-start | bytes 6148
  214.9 6.8 %copy-start.11 = (f32[1,512]{1,0:T(1,128)S(1)}, f32[1,512]{1,0:T(1,128)}, u32[]{:S(2)}) copy-start(f32[1,512]{1,0:T(1,128)} %get-tuple-element.35) | copy-start | bytes 6148
  214.9 6.8 %copy-start.12 = (f32[1,512]{1,0:T(1,128)S(1)}, f32[1,512]{1,0:T(1,128)}, u32[]{:S(2)}) copy-start(f32[1,512]{1,0:T(1,128)} %get-tuple-element.36) | copy-start | bytes 6148
  214.9 6.8 %copy-start.13 = (f32[1,512]{1,0:T(1,128)S(1)}, f32[1,512]{1,0:T(1,128)}, u32[]{:S(2)}) copy-start(f32[1,512]{1,0:T(1,128)} %get-tuple-element.37) | copy-start | bytes 6148
  214.9 6.8 %copy-start.14 = (f32[1,512]{1,0:T(1,128)S(1)}, f32[1,512]{1,0:T(1,128)}, u32[]{:S(2)}) copy-start(f32[1,512]{1,0:T(1,128)} %get-tuple-element.38) | copy-start | bytes 6148
  214.9 6.8 %copy-start.15 = (f32[1,512]{1,0:T(1,128)S(1)}, f32[1,512]{1,0:T(1,128)}, u32[]{:S(2)}) copy-start(f32[1,512]{1,0:T(1,128)} %get-tuple-element.39) | copy-start | bytes 6148
  214.9 6.8 %copy-start.16 = (f32[1,512]{1,0:T(1,128)S(1)}, f32[1,512]{1,0:T(1,128)}, u32[]{:S(2)}) copy-start(f32[1,512]{1,0:T(1,128)} %get-tuple-element.40) | copy-start | bytes 6148
  215.0 6.8 %copy-start.17 = (f32[1,512]{1,0:T(1,128)S(1)}, f32[1,512]{1,0:T(1,128)}, u32[]{:S(2)}) copy-start(f32[1,512]{1,0:T(1,128)} %get-tuple-element.41) | copy-start | bytes 6148
  215.0 6.8 %copy-start.18 = (f32[1,512]{1,0:T(1,128)S(1)}, f32[1,512]{1,0:T(1,128)}, u32[]{:S(2)}) copy-start(f32[1,512]{1,0:T(1,128)} %get-tuple-element.11) | copy-start | bytes 6148
  215.0 6.8 %copy-start.19 = (f32[1,512]{1,0:T(1,128)S(1)}, f32[1,512]{1,0:T(1,128)}, u32[]{:S(2)}) copy-start(f32[1,512]{1,0:T(1,128)} %get-tuple-element.12) | copy-start | bytes 6148
  215.0 6.8 %copy-start.20 = (f32[1,512]{1,0:T(1,128)S(1)}, f32[1,512]{1,0:T(1,128)}, u32[]{:S(2)}) copy-start(f32[1,512]{1,0:T(1,128)} %get-tuple-element.13) | copy-start | bytes 6148
  215.0 6.8 %copy-start.21 = (f32[1,512]{1,0:T(1,128)S(1)}, f32[1,512]{1,0:T(1,128)}, u32[]{:S(2)}) copy-start(f32[1,512]{1,0:T(1,128)} %get-tuple-element.14) | copy-start | bytes 6148
  215.0 6.8 %copy-start.22 = (f32[1,512]{1,0:T(1,128)S(1)}, f32[1,512]{1,0:T(1,128)}, u32[]{:S(2)}) copy-start(f32[1,512]{1,0:T(1,128)} %get-tuple-element.15) | copy-start | bytes 6148
  215.0 6.8 %copy-start.23 = (f32[1,512]{1,0:T(1,128)S(1)}, f32[1,512]{1,0:T(1,128)}, u32[]{:S(2)}) copy-start(f32[1,512]{1,0:T(1,128)} %get-tuple-element.16) | copy-start | bytes 6148
  215.0 6.8 %copy-start.24 = (f32[1,512]{1,0:T(1,128)S(1)}, f32[1,512]{1,0:T(1,128)}, u32[]{:S(2)}) copy-start(f32[1,512]{1,0:T(1,128)} %get-tuple-element.17) | copy-start | bytes 6148
  215.0 6.8 %copy-start.25 = (f32[1,512]{1,0:T(1,128)S(1)}, f32[1,512]{1,0:T(1,128)}, u32[]{:S(2)}) copy-start(f32[1,512]{1,0:T(1,128)} %get-tuple-element.18) | copy-start | bytes 6148
  215.0 6.8 %copy-start.26 = (f32[1,512]{1,0:T(1,128)S(1)}, f32[1,512]{1,0:T(1,128)}, u32[]{:S(2)}) copy-start(f32[1,512]{1,0:T(1,128)} %get-tuple-element.19) | copy-start | bytes 6148
  215.1 6.8 %copy-start.27 = (f32[1,512]{1,0:T(1,128)S(1)}, f32[1,512]{1,0:T(1,128)}, u32[]{:S(2)}) copy-start(f32[1,512]{1,0:T(1,128)} %get-tuple-element.20) | copy-start | bytes 6148
  215.1 6.8 %copy-start.28 = (f32[1,512]{1,0:T(1,128)S(1)}, f32[1,512]{1,0:T(1,128)}, u32[]{:S(2)}) copy-start(f32[1,512]{1,0:T(1,128)} %get-tuple-element.21) | copy-start | bytes 6148
  215.1 6.8 %copy-start.29 = (f32[1,512]{1,0:T(1,128)S(1)}, f32[1,512]{1,0:T(1,128)}, u32[]{:S(2)}) copy-start(f32[1,512]{1,0:T(1,128)} %get-tuple-element.22) | copy-start | bytes 6148
  215.2 6.5 %collective-permute-start = (f32[30,512]{1,0:T(8,128)S(1)}, f32[30,512]{1,0:T(8,128)S(1)}, u32[]{:S(2)}, u32[]{:S(2)}) collective-permute-start(f32[30,512]{1,0:T(8,128)S(1)} %slice.257), channel_id=1, source_target_pairs={{4,0},{8,4},{12,8},{16,12},{20,16},{24,20},{28,24},{5,1},{9,5},{13... | collective-permute-start | bytes 184328 | tf_op jit(solution)/shard_map/ppermute | solution.py:10
  (19 other events, 84.2 us)
Sparse Core Ops, SparseCore 0:
  33.8 21.5 all-gather.4
  57.0 22.5 all-gather.2
  88.7 51.3 all-reduce.2
  198.1 66.5 reduce-scatter.1
where the time goes:
time: 274 us; the launch traced here: 273 us
  waiting for transfers between devices  163 us (59%)
  blocking collectives  45.5 us (17%)
  matrix products  33.1 us (12%)
  between operations  14.5 us (5%)
  starting transfers between devices  6.96 us (3%)
  other arithmetic  6.52 us (2%)
  local copies, waits for them, and re-layouts  3.94 us (1%)
    psum x1, waiting for transfers between devices, shards(): summed = lax.psum(partial_value.astype(jnp.bfloat16), 'tp')  51.5 us
    all_to_all x1, waiting for transfers between devices, shards(): lax.all_to_all(summed.reshape(experts, capacity, model_width), 'sp', spli...  47.7 us
    reduce_scatter x1, waiting for transfers between devices, shards(): lax.psum_scatter(lax.dot_general(mixer_grad, act_conv, contract_first, pr...  40.9 us
    all_to_all x1, blocking collectives, shards(): lax.all_to_all(sent_rows, 'sp', split_axis=0, concat_axis=0, tiled=True)  21.7 us
    all_gather x1, waiting for transfers between devices, shards(): lax.all_gather(shared_rows[1], 'tp', axis=1, tiled=True)  17.9 us
    all_to_all x1, blocking collectives, shards(): lax.all_to_all(sent_grad, 'sp', split_axis=0, concat_axis=0, tiled=True)  17.6 us
    psum x1, blocking collectives, shards(): lax.psum((jnp.sum(norm_output_gradient, axis=1), jnp.sum(norm_output_grad...  6.16 us
    all_to_all x1, starting transfers between devices, shards(): lax.all_to_all(summed.reshape(experts, capacity, model_width), 'sp', spli...  5.51 us
  transfers between devices with their start and end apart: 6, of which 6 were waited for; matrix products, arithmetic and copies ran while one was open for 9% of the time, Pallas kernels for 0%

commit v1 on v0

--- a/solution.py
+++ b/solution.py
@@ -102,9 +102,13 @@
     partial_value = lax.dot_general(
         grad_gpre, w_first, contract_last, preferred_element_type=jnp.float32
     ) + lax.dot_general(grad_upre, w_third, contract_last, preferred_element_type=jnp.float32)
-    summed = lax.psum(partial_value.astype(jnp.bfloat16), "tp")
+    share = model_width // groups
+    partial_groups = jnp.transpose(
+        partial_value.astype(jnp.bfloat16).reshape(-1, groups, share), (1, 0, 2)
+    )
+    summed = lax.psum_scatter(partial_groups, "tp", scatter_dimension=0, tiled=False)
     home_rows = lax.all_to_all(
-        summed.reshape(experts, capacity, model_width),
+        summed.reshape(experts, capacity, share),
         "sp",
         split_axis=0,
         concat_axis=0,
@@ -112,23 +116,30 @@
     )
     returned = lax.dot_general(
         full_table,
-        home_rows.reshape(-1, model_width),
+        home_rows.reshape(-1, share),
         contract_first,
         preferred_element_type=jnp.float32,
     )
-    mixer_grad = (cotangent.astype(jnp.float32) + returned).astype(jnp.bfloat16)
+    own_cotangent = lax.dynamic_slice_in_dim(
+        cotangent, lax.axis_index("tp") * share, share, axis=1
+    )
+    mixer_share = (own_cotangent.astype(jnp.float32) + returned).astype(jnp.bfloat16)
+    mixer_grad = lax.all_gather(mixer_share, "tp", axis=1, tiled=True)
     normalized_input = saved_normalized.astype(jnp.float32)
     normalized_values = normalized_input * channel_norm_gain[None, :]
     gate_sig = jax.nn.sigmoid(normalized_values)
     act_conv = (normalized_values * gate_sig).astype(jnp.bfloat16)
-    grad_proj = lax.psum_scatter(
-        lax.dot_general(
-            mixer_grad, act_conv, contract_first, preferred_element_type=jnp.float32
-        ).astype(jnp.bfloat16),
-        "sp",
-        scatter_dimension=0,
-        tiled=True,
-    ).astype(jnp.float32)
+    every_act = lax.all_gather(act_conv, "sp", axis=0, tiled=True)
+    width_share = model_width // experts
+    sent_columns = jnp.stack(
+        [mixer_grad[:, i * width_share : (i + 1) * width_share] for i in range(experts)]
+    )
+    every_grad = lax.all_to_all(
+        sent_columns, "sp", split_axis=0, concat_axis=0, tiled=True
+    ).reshape(-1, width_share)
+    grad_proj = lax.dot_general(
+        every_grad, every_act, contract_first, preferred_element_type=jnp.float32
+    )
     grad_act = lax.dot_general(
         mixer_grad, proj_weight, contract_last, preferred_element_type=jnp.float32
     )

time: 274 us -> 204 us (0.74)
  waiting for transfers between devices: 163 us -> 75.5 us
  blocking collectives: 45.5 us -> 52.8 us
  local copies, waits for them, and re-layouts: 3.94 us -> 11.2 us
  starting transfers between devices: 6.96 us -> 11 us
    psum x1 -> x0, waiting for transfers between devices: 51.5 us -> none  [shards(): summed = lax.psum(partial_value.astype(jnp.bfloat16), 'tp')]
    all_to_all x1 -> x2, waiting for transfers between devices: 47.7 us -> 7.61 us  [the longest x1 6.78 us: shards(): lax.all_to_all(summed.reshape(experts, capacity, share), 'sp', split_axis...]
    all_gather x0 -> x1, waiting for transfers between devices: none -> 15.7 us  [shards(): every_act = lax.all_gather(act_conv, 'sp', axis=0, tiled=True)]
    reduce_scatter x1, waiting for transfers between devices: 40.9 us -> 29.2 us  [shards(): lax.psum_scatter(partial_groups, 'tp', scatter_dimension=0, tiled=False)]
    all_gather x0 -> x1, blocking collectives: none -> 6.5 us  [shards(): mixer_grad = lax.all_gather(mixer_share, 'tp', axis=1, tiled=True)]
    unnamed x91 -> x86, local copies, waits for them, and re-layouts: 1.77 us -> 6.86 us
    all_to_all x1 -> x2, starting transfers between devices: 5.51 us -> 9.51 us  [the longest x1 5.51 us: shards(): lax.all_to_all(summed.reshape(experts, capacity, share), 'sp', split_axis...]
  transfers between devices with their start and end apart: 6 -> 7, of which waited for: 6 -> 7; matrix products, arithmetic and copies ran while one was open for 9% -> 14% of each run, Pallas kernels for 0% -> 0%
where the time goes in v1:
time: 204 us
  waiting for transfers between devices  75.5 us (37%)
  blocking collectives  52.8 us (26%)
  matrix products  33.4 us (16%)
  between operations  14.4 us (7%)
  local copies, waits for them, and re-layouts  11.2 us (5%)
  starting transfers between devices  11 us (5%)
  other arithmetic  5.37 us (3%)
    reduce_scatter x1, waiting for transfers between devices, shards(): lax.psum_scatter(partial_groups, 'tp', scatter_dimension=0, tiled=False)  29.2 us
    all_to_all x1, blocking collectives, shards(): lax.all_to_all(sent_rows, 'sp', split_axis=0, concat_axis=0, tiled=True)  21.7 us
    all_gather x1, waiting for transfers between devices, shards(): lax.all_gather(shared_rows[1], 'tp', axis=1, tiled=True)  17.9 us
    all_to_all x1, blocking collectives, shards(): lax.all_to_all(sent_grad, 'sp', split_axis=0, concat_axis=0, tiled=True)  17.6 us
    all_gather x1, waiting for transfers between devices, shards(): every_act = lax.all_gather(act_conv, 'sp', axis=0, tiled=True)  15.7 us
    psum x1, blocking collectives, shards(): lax.psum((jnp.sum(norm_output_gradient, axis=1), jnp.sum(norm_output_grad...  6.96 us
    unnamed x86, local copies, waits for them, and re-layouts  6.86 us
    all_to_all x1, waiting for transfers between devices, shards(): lax.all_to_all(summed.reshape(experts, capacity, share), 'sp', split_axis...  6.78 us
  transfers between devices with their start and end apart: 7, of which 7 were waited for; matrix products, arithmetic and copies ran while one was open for 14% of the time, Pallas kernels for 0%

profile of v1, /device:TPU:0, one launch (start us, length us, event | category | flops | bytes accessed | tf_op | source)
XLA Modules:
  0.0 203.6 jit_solution(10553835263983900989)
XLA Ops:
  7.3 0.9 copy.33
  9.8 0.7 multiply_add_fusion
  10.6 1.3 convolution_convert_fusion.3
  11.9 21.7 %all_to_all.20 = bf16[8,16,2048]{2,1,0:T(8,128)(2,1)} all-to-all(bf16[8,16,2048]{2,1,0:T(8,128)(2,1)S(1)} %bitcast.130), channel_id=1, replica_groups=mesh['sp'=8,'tp'=4] {'sp'}, dimensions={0} | all-to-all | bytes 1048576 | tf_op jit(solution)/shard_map/all_to_all | solution.py:64
  34.2 17.6 %all_to_all.21 = bf16[8,16,2048]{2,1,0:T(8,128)(2,1)} all-to-all(bf16[8,16,2048]{2,1,0:T(8,128)(2,1)S(1)} %bitcast.129), channel_id=1, replica_groups=mesh['sp'=8,'tp'=4] {'sp'}, dimensions={0} | all-to-all | bytes 1048576 | tf_op jit(solution)/shard_map/all_to_all | solution.py:65
  51.9 3.5 %all-gather.6.cloned.1.call-done = bf16[8,64,2048]{2,1,0:T(8,128)(2,1)} async-done(((bf16[8,16,2048]{2,1,0:T(8,128)(2,1)}), bf16[8,64,2048]{2,1,0:T(8,128)(2,1)}) %all-gather.6.cloned.1.call-update) | async-done | bytes 2097168 | tf_op jit(solution)/shard_map/all_gather | solution.py:68
  55.4 4.0 %fusion.6 = f32[512,512]{1,0:T(8,128)} fusion(bf16[512,2048]{1,0:T(8,128)(2,1)} %bitcast.164, bf16[1,2048,512]{2,1,0:T(8,128)(2,1)S(1)} %copy-done), kind=kOutput, calls=%fused_computation.42 | convolution fusion | flops 1073741824 | bytes 5242880 | tf_op jit(solution)/shard_map/dot_general | solution.py:81
  59.4 2.3 %fusion.9 = f32[512,512]{1,0:T(8,128)} fusion(bf16[512,2048]{1,0:T(8,128)(2,1)S(1)} %bitcast.167, bf16[1,2048,512]{2,1,0:T(8,128)(2,1)S(1)} %copy-done.1), kind=kOutput, calls=%fused_computation.45 | convolution fusion | flops 1073741824 | bytes 5242880 | tf_op jit(solution)/shard_map/dot_general | solution.py:82
  61.7 17.9 %all-gather.4.cloned.1.call-done = bf16[8,64,2048]{2,1,0:T(8,128)(2,1)} async-done(((bf16[8,16,2048]{2,1,0:T(8,128)(2,1)}), bf16[8,64,2048]{2,1,0:T(8,128)(2,1)}) %all-gather.4.cloned.1.call-update) | async-done | bytes 2097168 | tf_op jit(solution)/shard_map/all_gather | solution.py:69
  79.6 4.4 %multiply_convert_fusion.1 = (bf16[512,512]{1,0:T(8,128)(2,1)S(1)}, bf16[512,512]{1,0:T(8,128)(2,1)S(1)}) fusion(f32[512,512]{1,0:T(8,128)} %fusion.6, f32[512,512]{1,0:T(8,128)} %fusion.9, bf16[512,2048]{1,0:T(8,128)(2,1)} %bitcast.168, bf16[1,512,2048]{2,1,0:T(8,128)(2,1)} %param.23), kind=kOutput, calls=%fused_computation.55 | convolution fusion | flops 1077149696 | bytes 7340032 | tf_op jit(solution)/shard_map/dot_general | solution.py:89
  84.0 1.3 fusion.4
  85.7 1.3 add_convert_fusion
  87.0 1.5 copy.39
  88.6 0.8 copy-done.6
  90.7 29.2 %reduce-scatter.2.cloned.1.call-done = bf16[1,512,512]{2,1,0:T(8,128)(2,1)} async-done(((bf16[4,512,512]{2,1,0:T(8,128)(2,1)}), bf16[1,512,512]{2,1,0:T(8,128)(2,1)}) %reduce-scatter.2.cloned.1.call-update) | async-done | bytes 524304 | tf_op jit(solution)/shard_map/reduce_scatter | solution.py:109
  119.9 5.5 %all-to-all-start.2 = ((bf16[8,64,512]{2,1,0:T(8,128)(2,1)}), bf16[8,64,512]{2,1,0:T(8,128)(2,1)S(1)}, u32[]{:S(2)}, u32[]{:S(2)}) async-start(bf16[8,64,512]{2,1,0:T(8,128)(2,1)} %bitcast.132), calls=%async_computation.3 | async-start | bytes 1048576 | tf_op jit(solution)/shard_map/all_to_all | solution.py:110
  125.8 4.4 %fusion.1 = bf16[1,2048,512]{2,1,0:T(8,128)(2,1)} fusion(bf16[512,2048]{1,0:T(8,128)(2,1)} %bitcast.165, bf16[512,512]{1,0:T(8,128)(2,1)} %copy-done.4), kind=kOutput, calls=%fused_computation.34 | convolution fusion | flops 1074790400 | bytes 4718592 | tf_op jit(solution)/shard_map/dot_general | solution.py:99
  130.3 2.7 %fusion.2 = bf16[1,512,2048]{2,1,0:T(8,128)(2,1)} fusion(bf16[512,2048]{1,0:T(8,128)(2,1)S(1)} %bitcast.169, f32[512,512]{1,0:T(8,128)S(1)} %copy-done.38, f32[512,512]{1,0:T(8,128)S(1)} %copy-done.37), kind=kOutput, calls=%fused_computation.35 | convolution fusion | flops 1076363264 | bytes 6291456 | tf_op jit(solution)/shard_map/dot_general | solution.py:86
  133.0 6.8 %all-to-all-done.2 = bf16[8,64,512]{2,1,0:T(8,128)(2,1)S(1)} async-done(((bf16[8,64,512]{2,1,0:T(8,128)(2,1)}), bf16[8,64,512]{2,1,0:T(8,128)(2,1)S(1)}, u32[]{:S(2)}, u32[]{:S(2)}) %all-to-all-start.2) | async-done | bytes 524320 | tf_op jit(solution)/shard_map/all_to_all | solution.py:110
  139.7 1.2 fusion.15
  140.9 6.5 %all_gather.14 = bf16[128,2048]{1,0:T(8,128)(2,1)S(1)} all-gather(bf16[128,512]{1,0:T(8,128)(2,1)S(1)} %fusion.15), channel_id=1, replica_groups=mesh['sp'=8,'tp'=4] {'tp'}, dimensions={1}, use_global_device_ids=true | all-gather | bytes 655360 | tf_op jit(solution)/shard_map/all_gather | solution.py:127
  148.1 3.6 %fusion.132 = (f32[128]{0:T(128)}, f32[128]{0:T(128)}, bf16[128,512]{1,0:T(8,128)(2,1)}, f32[128,512]{1,0:T(8,128)S(1)}) fusion(bf16[128,512]{1,0:T(8,128)(2,1)S(1)} %copy-done.5, f32[512]{0:T(512)} %param.18, bf16[128,2048]{1,0:T(8,128)(2,1)S(1)} %all_gather.14, bf16[512,2048]{1,0:T(8,128)(2,1)} %param.20), kind=kOutput, calls=%fused_computation.228 | convolution fusion | flops 269483776 | bytes 3148800 | tf_op jit(solution)/shard_map/dot_general | solution.py:143
  156.2 4.0 %all-to-all-start.3 = ((bf16[8,128,256]{2,1,0:T(8,128)(2,1)}), bf16[8,128,256]{2,1,0:T(8,128)(2,1)S(1)}, u32[]{:S(2)}, u32[]{:S(2)}) async-start(bf16[8,128,256]{2,1,0:T(8,128)(2,1)} %fusion.120), calls=%async_computation.4 | async-start | bytes 1048576 | tf_op jit(solution)/shard_map/all_to_all | solution.py:137
  160.2 7.0 %all-reduce = (f32[128]{0:T(128)}, f32[128]{0:T(128)}) all-reduce(f32[128]{0:T(128)} %get-tuple-element.6, f32[128]{0:T(128)} %get-tuple-element.5), channel_id=1, replica_groups=mesh['sp'=8,'tp'=4] {'tp'}, use_global_device_ids=true, to_apply=%region_10.11 | all-reduce | flops 256 | bytes 2048 | tf_op jit(solution)/shard_map/psum | solution.py:152
  167.8 0.8 fusion.27
  168.9 1.3 collective-permute-start
  170.2 4.2 %fusion = bf16[1,2048,512]{2,1,0:T(8,128)(2,1)} fusion(bf16[512,2048]{1,0:T(8,128)(2,1)} %bitcast.166, bf16[512,512]{1,0:T(8,128)(2,1)S(1)} %get-tuple-element.10), kind=kOutput, calls=%fused_computation.33 | convolution fusion | flops 1074790400 | bytes 4718592 | tf_op jit(solution)/shard_map/dot_general | solution.py:96
  174.4 1.5 collective-permute-done
  176.1 2.0 fusion.32
  178.1 0.8 all-to-all-done.3
  178.9 15.7 %all-gather.8.cloned.1.call-done = bf16[1024,512]{1,0:T(8,128)(2,1)} async-done(((bf16[128,512]{1,0:T(8,128)(2,1)}), bf16[1024,512]{1,0:T(8,128)(2,1)}) %all-gather.8.cloned.1.call-update) | async-done | bytes 1048592 | tf_op jit(solution)/shard_map/all_gather | solution.py:132
  194.6 2.5 %fusion.135 = f32[256,512]{1,0:T(8,128)} fusion(bf16[1024,256]{1,0:T(8,128)(2,1)S(1)} %bitcast.131, bf16[1024,512]{1,0:T(8,128)(2,1)} %all-gather.8.cloned.1.call-done), kind=kOutput, calls=%fused_computation.231 | convolution fusion | flops 268435456 | bytes 2097152 | tf_op jit(solution)/shard_map/dot_general | solution.py:140
  (117 shorter events, 10.4 us)
Async XLA Ops:
  7.2 48.3 %copy-start = (bf16[1,2048,512]{2,1,0:T(8,128)(2,1)S(1)}, bf16[1,2048,512]{2,1,0:T(8,128)(2,1)}, u32[]{:S(2)}) copy-start(bf16[1,2048,512]{2,1,0:T(8,128)(2,1)} %param.21) | copy-start | bytes 6291460
  7.2 26.5 %copy-start.34 = (f32[128,2]{0,1:T(2,128)S(1)}, f32[128,2]{0,1:T(2,128)}, u32[]{:S(2)}) copy-start(f32[128,2]{0,1:T(2,128)} %param.15) | copy-start | bytes 3076
  7.2 26.7 %copy-start.3 = (bf16[128,2048]{1,0:T(8,128)(2,1)S(1)}, bf16[128,2048]{1,0:T(8,128)(2,1)}, u32[]{:S(2)}) copy-start(bf16[128,2048]{1,0:T(8,128)(2,1)} %param.12) | copy-start | bytes 1572868
  7.2 48.2 %all-gather.6.cloned.1.call-start = ((), (), s32[]{:S(2)}) async-start(), calls=%async_computation.6 | async-start | bytes 2621440 | tf_op jit(solution)/shard_map/all_gather | solution.py:68
  33.7 45.9 %all-gather.4.cloned.1.call-start = ((), (), s32[]{:S(2)}) async-start(), calls=%async_computation.5 | async-start | bytes 2621440 | tf_op jit(solution)/shard_map/all_gather | solution.py:69
  51.9 68.0 %reduce-scatter.2.cloned.1.call-start = ((), (), s32[]{:S(2)}) async-start(), calls=%async_computation.7 | async-start | bytes 2621440 | tf_op jit(solution)/shard_map/reduce_scatter | solution.py:109
  119.9 19.8 %all-to-all-start.2 = ((bf16[8,64,512]{2,1,0:T(8,128)(2,1)}), bf16[8,64,512]{2,1,0:T(8,128)(2,1)S(1)}, u32[]{:S(2)}, u32[]{:S(2)}) async-start(bf16[8,64,512]{2,1,0:T(8,128)(2,1)} %bitcast.132), calls=%async_computation.3 | async-start | bytes 1048576 | tf_op jit(solution)/shard_map/all_to_all | solution.py:110
  125.4 69.2 %all-gather.8.cloned.1.call-start = ((), (), s32[]{:S(2)}) async-start(), calls=%async_computation.8 | async-start | bytes 1179648 | tf_op jit(solution)/shard_map/all_gather | solution.py:132
  130.2 17.8 %copy-start.5 = (bf16[128,512]{1,0:T(8,128)(2,1)S(1)}, bf16[128,512]{1,0:T(8,128)(2,1)}, u32[]{:S(2)}) copy-start(bf16[128,512]{1,0:T(8,128)(2,1)} %param.16) | copy-start | bytes 393220
  156.2 22.8 %all-to-all-start.3 = ((bf16[8,128,256]{2,1,0:T(8,128)(2,1)}), bf16[8,128,256]{2,1,0:T(8,128)(2,1)S(1)}, u32[]{:S(2)}, u32[]{:S(2)}) async-start(bf16[8,128,256]{2,1,0:T(8,128)(2,1)} %fusion.120), calls=%async_computation.4 | async-start | bytes 1048576 | tf_op jit(solution)/shard_map/all_to_all | solution.py:137
  168.6 7.3 %copy-start.7 = (f32[1,512]{1,0:T(1,128)S(1)}, f32[1,512]{1,0:T(1,128)}, u32[]{:S(2)}) copy-start(f32[1,512]{1,0:T(1,128)} %get-tuple-element.35) | copy-start | bytes 6148
  168.6 7.3 %copy-start.8 = (f32[1,512]{1,0:T(1,128)S(1)}, f32[1,512]{1,0:T(1,128)}, u32[]{:S(2)}) copy-start(f32[1,512]{1,0:T(1,128)} %get-tuple-element.36) | copy-start | bytes 6148
  168.6 7.3 %copy-start.9 = (f32[1,512]{1,0:T(1,128)S(1)}, f32[1,512]{1,0:T(1,128)}, u32[]{:S(2)}) copy-start(f32[1,512]{1,0:T(1,128)} %get-tuple-element.37) | copy-start | bytes 6148
  168.6 7.3 %copy-start.10 = (f32[1,512]{1,0:T(1,128)S(1)}, f32[1,512]{1,0:T(1,128)}, u32[]{:S(2)}) copy-start(f32[1,512]{1,0:T(1,128)} %get-tuple-element.38) | copy-start | bytes 6148
  168.6 7.3 %copy-start.11 = (f32[1,512]{1,0:T(1,128)S(1)}, f32[1,512]{1,0:T(1,128)}, u32[]{:S(2)}) copy-start(f32[1,512]{1,0:T(1,128)} %get-tuple-element.39) | copy-start | bytes 6148
  168.7 7.3 %copy-start.12 = (f32[1,512]{1,0:T(1,128)S(1)}, f32[1,512]{1,0:T(1,128)}, u32[]{:S(2)}) copy-start(f32[1,512]{1,0:T(1,128)} %get-tuple-element.40) | copy-start | bytes 6148
  168.7 7.3 %copy-start.13 = (f32[1,512]{1,0:T(1,128)S(1)}, f32[1,512]{1,0:T(1,128)}, u32[]{:S(2)}) copy-start(f32[1,512]{1,0:T(1,128)} %get-tuple-element.41) | copy-start | bytes 6148
  168.7 7.3 %copy-start.14 = (f32[1,512]{1,0:T(1,128)S(1)}, f32[1,512]{1,0:T(1,128)}, u32[]{:S(2)}) copy-start(f32[1,512]{1,0:T(1,128)} %get-tuple-element.42) | copy-start | bytes 6148
  168.7 7.3 %copy-start.15 = (f32[1,512]{1,0:T(1,128)S(1)}, f32[1,512]{1,0:T(1,128)}, u32[]{:S(2)}) copy-start(f32[1,512]{1,0:T(1,128)} %get-tuple-element.12) | copy-start | bytes 6148
  168.7 7.3 %copy-start.16 = (f32[1,512]{1,0:T(1,128)S(1)}, f32[1,512]{1,0:T(1,128)}, u32[]{:S(2)}) copy-start(f32[1,512]{1,0:T(1,128)} %get-tuple-element.13) | copy-start | bytes 6148
  168.7 7.3 %copy-start.17 = (f32[1,512]{1,0:T(1,128)S(1)}, f32[1,512]{1,0:T(1,128)}, u32[]{:S(2)}) copy-start(f32[1,512]{1,0:T(1,128)} %get-tuple-element.14) | copy-start | bytes 6148
  168.7 7.3 %copy-start.18 = (f32[1,512]{1,0:T(1,128)S(1)}, f32[1,512]{1,0:T(1,128)}, u32[]{:S(2)}) copy-start(f32[1,512]{1,0:T(1,128)} %get-tuple-element.15) | copy-start | bytes 6148
  168.7 7.3 %copy-start.19 = (f32[1,512]{1,0:T(1,128)S(1)}, f32[1,512]{1,0:T(1,128)}, u32[]{:S(2)}) copy-start(f32[1,512]{1,0:T(1,128)} %get-tuple-element.16) | copy-start | bytes 6148
  168.7 7.3 %copy-start.20 = (f32[1,512]{1,0:T(1,128)S(1)}, f32[1,512]{1,0:T(1,128)}, u32[]{:S(2)}) copy-start(f32[1,512]{1,0:T(1,128)} %get-tuple-element.17) | copy-start | bytes 6148
  168.7 7.3 %copy-start.21 = (f32[1,512]{1,0:T(1,128)S(1)}, f32[1,512]{1,0:T(1,128)}, u32[]{:S(2)}) copy-start(f32[1,512]{1,0:T(1,128)} %get-tuple-element.18) | copy-start | bytes 6148
  168.8 7.3 %copy-start.22 = (f32[1,512]{1,0:T(1,128)S(1)}, f32[1,512]{1,0:T(1,128)}, u32[]{:S(2)}) copy-start(f32[1,512]{1,0:T(1,128)} %get-tuple-element.19) | copy-start | bytes 6148
  168.8 7.3 %copy-start.23 = (f32[1,512]{1,0:T(1,128)S(1)}, f32[1,512]{1,0:T(1,128)}, u32[]{:S(2)}) copy-start(f32[1,512]{1,0:T(1,128)} %get-tuple-element.20) | copy-start | bytes 6148
  168.8 7.3 %copy-start.24 = (f32[1,512]{1,0:T(1,128)S(1)}, f32[1,512]{1,0:T(1,128)}, u32[]{:S(2)}) copy-start(f32[1,512]{1,0:T(1,128)} %get-tuple-element.21) | copy-start | bytes 6148
  168.8 7.3 %copy-start.25 = (f32[1,512]{1,0:T(1,128)S(1)}, f32[1,512]{1,0:T(1,128)}, u32[]{:S(2)}) copy-start(f32[1,512]{1,0:T(1,128)} %get-tuple-element.22) | copy-start | bytes 6148
  168.8 7.3 %copy-start.26 = (f32[1,512]{1,0:T(1,128)S(1)}, f32[1,512]{1,0:T(1,128)}, u32[]{:S(2)}) copy-start(f32[1,512]{1,0:T(1,128)} %get-tuple-element.23) | copy-start | bytes 6148
  168.8 7.3 %copy-start.27 = (f32[1,512]{1,0:T(1,128)S(1)}, f32[1,512]{1,0:T(1,128)}, u32[]{:S(2)}) copy-start(f32[1,512]{1,0:T(1,128)} %get-tuple-element.24) | copy-start | bytes 6148
  168.9 7.0 %collective-permute-start = (f32[30,512]{1,0:T(8,128)S(1)}, f32[30,512]{1,0:T(8,128)S(1)}, u32[]{:S(2)}, u32[]{:S(2)}) collective-permute-start(f32[30,512]{1,0:T(8,128)S(1)} %slice.289), channel_id=1, source_target_pairs={{4,0},{8,4},{12,8},{16,12},{20,16},{24,20},{28,24},{5,1},{9,5},{13... | collective-permute-start | bytes 184328 | tf_op jit(solution)/shard_map/ppermute | solution.py:10
  (14 other events, 68.9 us)
Sparse Core Ops, SparseCore 0:
  33.8 21.5 all-gather.5
  57.0 22.5 all-gather.3
  88.7 31.1 reduce-scatter.1
  151.8 42.7 all-gather.7

commit v2 on v1

--- a/solution.py
+++ b/solution.py
@@ -1,6 +1,10 @@
+import functools
+
 import jax
 import jax.numpy as jnp
 from jax import lax
+from jax.experimental import pallas as pl
+from jax.experimental.pallas import tpu as pltpu
 from jax.sharding import PartitionSpec as P
 
 
@@ -27,6 +31,136 @@
     dispatch = jnp.any(matched, axis=2).astype(jnp.bfloat16)
     slot_weight = jnp.sum(jnp.where(matched, route_weight[None, :, :], 0.0), axis=(1, 2))
     return (dispatch, slot_weight)
+
+
+def remote(source, target, send_sem, recv_sem, device):
+    return pltpu.make_async_remote_copy(
+        src_ref=source,
+        dst_ref=target,
+        send_sem=send_sem,
+        recv_sem=recv_sem,
+        device_id=device,
+        device_id_type=pl.DeviceIdType.MESH,
+    )
+
+
+def dispatch_kernel(experts, groups, *refs):
+    sent = refs[:2]
+    held = refs[2:4]
+    local_sem, far_send, far_recv, row_send, row_recv, pair_send, pair_recv = refs[4:]
+    mine = lax.axis_index("sp")
+    place = lax.axis_index("tp")
+    chips = groups // 2
+    chip, core = place // 2, place % 2
+    sibling = chip * 2 + 1 - core
+
+    def at_chip(step):
+        return ((chip + step) % chips) * 2 + core
+
+    barrier = pltpu.get_barrier_semaphore()
+
+    def greet(step, carry):
+        pl.semaphore_signal(barrier, inc=1, device_id=((mine + step) % experts, place),
+                            device_id_type=pl.DeviceIdType.MESH)
+        return carry
+
+    lax.fori_loop(1, experts, greet, 0)
+    for step in range(1, chips):
+        pl.semaphore_signal(barrier, inc=1, device_id=(mine, at_chip(step)),
+                            device_id_type=pl.DeviceIdType.MESH)
+    pl.semaphore_signal(barrier, inc=1, device_id=(mine, sibling),
+                        device_id_type=pl.DeviceIdType.MESH)
+    pl.semaphore_wait(barrier, experts - 1 + chips)
+
+    def far(a, step):
+        peer = (mine + step) % experts
+        return remote(sent[a].at[peer], held[a].at[mine, place],
+                      far_send.at[a, step], far_recv.at[a, step], (peer, place))
+
+    def row(a, step, hop):
+        source = (mine + experts - step) % experts
+        block = held[a].at[source, place]
+        return remote(block, block, row_send.at[a, step, hop], row_recv.at[a, step, hop],
+                      (mine, at_chip(hop)))
+
+    def pair(a, step, hop):
+        source = (mine + experts - step) % experts
+        block = held[a].at[source, at_chip(chips - hop)]
+        return remote(block, block, pair_send.at[a, step, hop], pair_recv.at[a, step, hop],
+                      (mine, sibling))
+
+    own = [
+        pltpu.make_async_copy(sent[a].at[mine], held[a].at[mine, place], local_sem.at[a])
+        for a in range(2)
+    ]
+    for a in range(2):
+        own[a].start()
+    for a in range(2):
+        def start_far(step, carry, a=a):
+            far(a, step).start()
+            return carry
+
+        lax.fori_loop(1, experts, start_far, 0)
+
+    def pass_on(a, step):
+        for hop in range(1, chips):
+            row(a, step, hop).start()
+        pair(a, step, 0).start()
+
+    def pass_rows(a, step):
+        for hop in range(1, chips):
+            row(a, step, hop).wait_recv()
+            pair(a, step, hop).start()
+
+    for a in range(2):
+        own[a].wait()
+        pass_on(a, 0)
+    for a in range(2):
+        def arrive(step, carry, a=a):
+            far(a, step).wait_recv()
+            pass_on(a, step)
+            pass_rows(a, step - 1)
+            return carry
+
+        lax.fori_loop(1, experts, arrive, 0)
+        pass_rows(a, experts - 1)
+    for a in range(2):
+        def finish(step, carry, a=a):
+            for hop in range(chips):
+                pair(a, step, hop).wait()
+                if hop:
+                    row(a, step, hop).wait_send()
+            return carry
+
+        lax.fori_loop(0, experts, finish, 0)
+
+        def finish_far(step, carry, a=a):
+            far(a, step).wait_send()
+            return carry
+
+        lax.fori_loop(1, experts, finish_far, 0)
+
+
+def dispatch_blocks(rows, grads, groups):
+    experts, span, width = rows.shape
+    chips = groups // 2
+    full = jax.ShapeDtypeStruct((experts, groups, span, width), rows.dtype)
+    dma = pltpu.SemaphoreType.DMA
+    return pl.pallas_call(
+        functools.partial(dispatch_kernel, experts, groups),
+        out_shape=(full, full),
+        in_specs=[pl.BlockSpec(memory_space=pltpu.VMEM)] * 2,
+        out_specs=[pl.BlockSpec(memory_space=pltpu.VMEM)] * 2,
+        scratch_shapes=[dma((2,))]
+        + [dma((2, experts))] * 2
+        + [dma((2, experts, chips))] * 4,
+        compiler_params=pltpu.CompilerParams(
+            collective_id=0, has_side_effects=True, vmem_limit_bytes=24 * 2**20
+        ),
+        cost_estimate=pl.CostEstimate(
+            flops=0, bytes_accessed=40 * full.size, transcendentals=0
+        ),
+    )(rows, grads)
 
 
 def shards(
@@ -60,14 +194,13 @@
     ).astype(jnp.bfloat16)
     sent_rows = sent_rows.reshape(experts, slot_span, model_width)
     sent_grad = sent_grad.reshape(experts, slot_span, model_width)
-    shared_rows = (
-        lax.all_to_all(sent_rows, "sp", split_axis=0, concat_axis=0, tiled=True),
-        lax.all_to_all(sent_grad, "sp", split_axis=0, concat_axis=0, tiled=True),
-    )
-    routed_rows, routed_grad = (
-        lax.all_gather(shared_rows[0], "tp", axis=1, tiled=True),
-        lax.all_gather(shared_rows[1], "tp", axis=1, tiled=True),
-    )
+    normalized_input = saved_normalized.astype(jnp.float32)
+    normalized_values = normalized_input * channel_norm_gain[None, :]
+    gate_sig = jax.nn.sigmoid(normalized_values)
+    act_conv = (normalized_values * gate_sig).astype(jnp.bfloat16)
+    act_conv, sent_rows = lax.optimization_barrier((act_conv, sent_rows))
+    every_act = lax.all_gather(act_conv, "sp", axis=0, tiled=True)
+    routed_rows, routed_grad = dispatch_blocks(sent_rows, sent_grad, groups)
     full_table, unused_weight = route_table(
         expert_ids, route_weight, 0, capacity, capacity, experts
     )
@@ -106,6 +239,7 @@
     partial_groups = jnp.transpose(
         partial_value.astype(jnp.bfloat16).reshape(-1, groups, share), (1, 0, 2)
     )
+    every_act, partial_groups = lax.optimization_barrier((every_act, partial_groups))
     summed = lax.psum_scatter(partial_groups, "tp", scatter_dimension=0, tiled=False)
     home_rows = lax.all_to_all(
         summed.reshape(experts, capacity, share),
@@ -125,14 +259,9 @@
     )
     mixer_share = (own_cotangent.astype(jnp.float32) + returned).astype(jnp.bfloat16)
     mixer_grad = lax.all_gather(mixer_share, "tp", axis=1, tiled=True)
-    normalized_input = saved_normalized.astype(jnp.float32)
-    normalized_values = normalized_input * channel_norm_gain[None, :]
-    gate_sig = jax.nn.sigmoid(normalized_values)
-    act_conv = (normalized_values * gate_sig).astype(jnp.bfloat16)
-    every_act = lax.all_gather(act_conv, "sp", axis=0, tiled=True)
     width_share = model_width // experts
-    sent_columns = jnp.stack(
-        [mixer_grad[:, i * width_share : (i + 1) * width_share] for i in range(experts)]
+    sent_columns = jnp.transpose(
+        mixer_grad.reshape(tok_rows, experts, width_share), (1, 0, 2)
     )
     every_grad = lax.all_to_all(
         sent_columns, "sp", split_axis=0, concat_axis=0, tiled=True

time: 204 us -> 170 us (0.83)
  Pallas kernels: 0 us -> 43.7 us
  blocking collectives: 52.8 us -> 13.2 us
  waiting for transfers between devices: 75.5 us -> 44.2 us
  matrix products: 33.4 us -> 25.5 us
  other arithmetic: 5.37 us -> 7.78 us
    pallas_call x0 -> x1, Pallas kernels: none -> 43.7 us  [dispatch_blocks(): pl.pallas_call(functools.partial(dispatch_kernel, experts, groups), out_s...]
    all_to_all x2 -> x0, blocking collectives: 39.3 us -> none  [the longest x1 21.7 us: shards(): lax.all_to_all(sent_rows, 'sp', split_axis=0, concat_axis=0, tiled=True)]
    all_gather x2 -> x0, waiting for transfers between devices: 21.4 us -> none  [the longest x1 17.9 us: shards(): lax.all_gather(shared_rows[1], 'tp', axis=1, tiled=True)]
    all_gather x1, waiting for transfers between devices: 15.7 us -> 0.01 us  [shards(): every_act = lax.all_gather(act_conv, 'sp', axis=0, tiled=True)]
    reduce_scatter x1, waiting for transfers between devices: 29.2 us -> 33.5 us  [shards(): lax.psum_scatter(partial_groups, 'tp', scatter_dimension=0, tiled=False)]
    dot_general x1, matrix products: 4.35 us -> 1.58 us  [shards(): lax.dot_general(routed_grad, w_second, contract_last, preferred_element_t...]
    dot_general x1, matrix products: 3.96 us -> 1.25 us  [shards(): jnp.dot(routed_rows, w_first, preferred_element_type=jnp.float32)]
    unnamed x86 -> x29, local copies, waits for them, and re-layouts: 6.86 us -> 4.34 us
  transfers between devices with their start and end apart: 7 -> 5, of which waited for: 7 -> 3; matrix products, arithmetic and copies ran while one was open for 14% -> 17% of each run, Pallas kernels for 0% -> 26%
where the time goes in v2:
time: 170 us; the launch traced here: 169 us
  waiting for transfers between devices  44.2 us (26%)
  Pallas kernels  43.7 us (26%)
  matrix products  25.5 us (15%)
  between operations  14.3 us (8%)
  blocking collectives  13.2 us (8%)
  starting transfers between devices  10.9 us (6%)
  local copies, waits for them, and re-layouts  9.22 us (5%)
  other arithmetic  7.78 us (5%)
    pallas_call x1, Pallas kernels, dispatch_blocks(): pl.pallas_call(functools.partial(dispatch_kernel, experts, groups), out_s...  43.7 us
    reduce_scatter x1, waiting for transfers between devices, shards(): lax.psum_scatter(partial_groups, 'tp', scatter_dimension=0, tiled=False)  33.5 us
    all_to_all x1, waiting for transfers between devices, shards(): lax.all_to_all(summed.reshape(experts, capacity, share), 'sp', split_axis...  6.83 us
    psum x1, blocking collectives, shards(): lax.psum((jnp.sum(norm_output_gradient, axis=1), jnp.sum(norm_output_grad...  6.72 us
    all_gather x1, blocking collectives, shards(): mixer_grad = lax.all_gather(mixer_share, 'tp', axis=1, tiled=True)  6.5 us
    all_to_all x1, starting transfers between devices, shards(): lax.all_to_all(summed.reshape(experts, capacity, share), 'sp', split_axis...  5.52 us
    dot_general x1, matrix products, shards(): lax.dot_general(routed_rows, grad_upre, contract_first, preferred_element...  4.43 us
    unnamed x29, local copies, waits for them, and re-layouts  4.34 us
  transfers between devices with their start and end apart: 5, of which 3 were waited for; matrix products, arithmetic and copies ran while one was open for 17% of the time, Pallas kernels for 26%

profile of v2, /device:TPU:0, one launch (start us, length us, event | category | flops | bytes accessed | tf_op | source)
XLA Modules:
  0.0 168.8 jit_solution(1275019702469023254)
XLA Ops:
  7.2 1.0 copy.35
  9.6 0.7 multiply_add_fusion
  10.6 1.3 convolution_convert_fusion.3
  12.0 1.6 fusion.23
  13.7 0.9 fusion.119
  14.8 43.7 %shard_map.155 = (bf16[8,4,16,2048]{3,2,1,0:T(8,128)(2,1)S(1)}, bf16[8,4,16,2048]{3,2,1,0:T(8,128)(2,1)S(1)}) custom-call(bf16[8,16,2048]{2,1,0:T(8,128)(2,1)S(1)} %bitcast.101, bf16[8,16,2048]{2,1,0:T(8,128)(2,1)S(1)} %bitcast.102), custom_call_target="tpu_custom_call" | custom-call | bytes 41943040 | tf_op jit(solution)/shard_map/pallas_call | solution.py:149
  58.6 1.2 fusion.6
  59.9 1.8 %copy-done.4 = bf16[1,2048,512]{2,1,0:T(8,128)(2,1)S(1)} copy-done((bf16[1,2048,512]{2,1,0:T(8,128)(2,1)S(1)}, bf16[1,2048,512]{2,1,0:T(8,128)(2,1)}, u32[]{:S(2)}) %copy-start.4) | copy-done | bytes 2097176
  61.7 1.2 fusion.9
  62.9 0.7 copy-done.9
  63.6 1.6 multiply_convert_fusion.1
  65.2 1.3 fusion.4
  66.5 1.3 add_convert_fusion
  67.8 1.5 copy.44
  69.4 0.8 copy-done.8
  70.9 4.2 %fusion = bf16[1,2048,512]{2,1,0:T(8,128)(2,1)} fusion(bf16[512,2048]{1,0:T(8,128)(2,1)} %bitcast.107, bf16[512,512]{1,0:T(8,128)(2,1)S(1)} %get-tuple-element.22), kind=kOutput, calls=%fused_computation.33 | convolution fusion | flops 1074790400 | bytes 4718592 | tf_op jit(solution)/shard_map/dot_general | solution.py:229
  75.1 33.5 %reduce-scatter.2.cloned.1.call-done = bf16[1,512,512]{2,1,0:T(8,128)(2,1)} async-done(((bf16[4,512,512]{2,1,0:T(8,128)(2,1)}), bf16[1,512,512]{2,1,0:T(8,128)(2,1)}) %reduce-scatter.2.cloned.1.call-update) | async-done | bytes 524304 | tf_op jit(solution)/shard_map/reduce_scatter | solution.py:243
  108.5 5.5 %all-to-all-start = ((bf16[8,64,512]{2,1,0:T(8,128)(2,1)}), bf16[8,64,512]{2,1,0:T(8,128)(2,1)S(1)}, u32[]{:S(2)}, u32[]{:S(2)}) async-start(bf16[8,64,512]{2,1,0:T(8,128)(2,1)} %bitcast.114), calls=%async_computation.1 | async-start | bytes 1048576 | tf_op jit(solution)/shard_map/all_to_all | solution.py:244
  114.4 4.4 %fusion.1 = bf16[1,2048,512]{2,1,0:T(8,128)(2,1)} fusion(bf16[512,2048]{1,0:T(8,128)(2,1)} %bitcast.108, bf16[512,512]{1,0:T(8,128)(2,1)} %copy-done.6), kind=kOutput, calls=%fused_computation.34 | convolution fusion | flops 1074790400 | bytes 4718592 | tf_op jit(solution)/shard_map/dot_general | solution.py:232
  118.8 2.7 %fusion.2 = bf16[1,512,2048]{2,1,0:T(8,128)(2,1)} fusion(bf16[512,2048]{1,0:T(8,128)(2,1)S(1)} %bitcast.104, f32[512,512]{1,0:T(8,128)S(1)} %copy-done.13, f32[512,512]{1,0:T(8,128)S(1)} %copy-done.11), kind=kOutput, calls=%fused_computation.35 | convolution fusion | flops 1076363264 | bytes 6291456 | tf_op jit(solution)/shard_map/dot_general | solution.py:219
  121.5 6.8 %all-to-all-done = bf16[8,64,512]{2,1,0:T(8,128)(2,1)S(1)} async-done(((bf16[8,64,512]{2,1,0:T(8,128)(2,1)}), bf16[8,64,512]{2,1,0:T(8,128)(2,1)S(1)}, u32[]{:S(2)}, u32[]{:S(2)}) %all-to-all-start) | async-done | bytes 524320 | tf_op jit(solution)/shard_map/all_to_all | solution.py:244
  128.6 6.5 %all_gather.7 = bf16[128,2048]{1,0:T(8,128)(2,1)S(1)} all-gather(bf16[128,512]{1,0:T(8,128)(2,1)S(1)} %fusion.15), channel_id=1, replica_groups=mesh['sp'=8,'tp'=4] {'tp'}, dimensions={1}, use_global_device_ids=true | all-gather | bytes 655360 | tf_op jit(solution)/shard_map/all_gather | solution.py:261
  135.1 0.8 copy.45
  136.0 4.0 %all-to-all-start.1 = ((bf16[8,128,256]{2,1,0:T(8,128)(2,1)}), bf16[8,128,256]{2,1,0:T(8,128)(2,1)S(1)}, u32[]{:S(2)}, u32[]{:S(2)}) async-start(bf16[8,128,256]{2,1,0:T(8,128)(2,1)} %bitcast.100), calls=%async_computation.2 | async-start | bytes 1048576 | tf_op jit(solution)/shard_map/all_to_all | solution.py:266
  140.0 3.1 %fusion.124 = (f32[128]{0:T(128)}, f32[128]{0:T(128)}, f32[128,512]{1,0:T(8,128)S(1)}) fusion(bf16[128,512]{1,0:T(8,128)(2,1)S(1)} %copy-done.7, f32[512]{0:T(512)} %param.18, bf16[128,2048]{1,0:T(8,128)(2,1)S(1)} %all_gather.7, bf16[512,2048]{1,0:T(8,128)(2,1)} %param.20), kind=kOutput, calls=%fused_computation.213 | convolution fusion | flops 269352704 | bytes 3017728 | tf_op jit(solution)/shard_map/dot_general | solution.py:272
  143.1 6.7 %all-reduce = (f32[128]{0:T(128)S(1)}, f32[128]{0:T(128)S(1)}) all-reduce(f32[128]{0:T(128)} %get-tuple-element.18, f32[128]{0:T(128)} %get-tuple-element.17), channel_id=1, replica_groups=mesh['sp'=8,'tp'=4] {'tp'}, use_global_device_ids=true, to_apply=%region_10.11 | all-reduce | flops 256 | bytes 2048 | tf_op jit(solution)/shard_map/psum | solution.py:281
  149.8 0.8 fusion.27
  150.6 1.3 collective-permute-start
  151.9 1.0 fusion.126
  152.9 3.8 %collective-permute-done = f32[30,512]{1,0:T(8,128)S(1)} collective-permute-done((f32[30,512]{1,0:T(8,128)S(1)}, f32[30,512]{1,0:T(8,128)S(1)}, u32[]{:S(2)}, u32[]{:S(2)}) %collective-permute-start) | collective-permute-done | bytes 61472 | tf_op jit(solution)/shard_map/ppermute | solution.py:14
  156.7 2.7 %fusion.32 = bf16[128,512]{1,0:T(8,128)(2,1)} fusion(f32[128,512]{1,0:T(8,128)S(1)} %fusion.27, f32[30,512]{1,0:T(8,128)S(1)} %collective-permute-done, f32[512]{0:T(512)S(1)} %bitcast.144, f32[512]{0:T(512)S(1)} %bitcast.145, f32[512]{0:T(512)S(1)} %bitcast.116, f32[512]{0:T(512)S(1)} %bitcast.117, f32[512]{0:T(512)S(1)} %bitcast.118, f32[512]{0:T(512)} %bitcast.119, ...), kind=kLoop, calls=%fused_computation.108 | loop fusion | flops 6029312 | bytes 518144 | tf_op jit(solution)/shard_map/convert_element_type | solution.py:301
  159.4 2.5 %fusion.127 = f32[256,512]{1,0:T(8,128)} fusion(bf16[1024,256]{1,0:T(8,128)(2,1)S(1)} %bitcast.113, bf16[1024,512]{1,0:T(8,128)(2,1)} %all-gather.2.cloned.1.call-done), kind=kOutput, calls=%fused_computation.216 | convolution fusion | flops 268435456 | bytes 2097152 | tf_op jit(solution)/shard_map/dot_general | solution.py:269
  (54 shorter events, 3.4 us)
Async XLA Ops:
  7.2 51.4 %copy-start = (bf16[1,2048,512]{2,1,0:T(8,128)(2,1)S(1)}, bf16[1,2048,512]{2,1,0:T(8,128)(2,1)}, u32[]{:S(2)}) copy-start(bf16[1,2048,512]{2,1,0:T(8,128)(2,1)} %param.21) | copy-start | bytes 6291460
  7.2 7.4 %copy-start.5 = (bf16[128,2048]{1,0:T(8,128)(2,1)S(1)}, bf16[128,2048]{1,0:T(8,128)(2,1)}, u32[]{:S(2)}) copy-start(bf16[128,2048]{1,0:T(8,128)(2,1)} %param.12) | copy-start | bytes 1572868
  7.2 62.2 %all-gather.2.cloned.1.call-start = ((), (), s32[]{:S(2)}) async-start(), calls=%async_computation.3 | async-start | bytes 1179648 | tf_op jit(solution)/shard_map/all_gather | solution.py:202
  13.6 94.9 %reduce-scatter.2.cloned.1.call-start = ((), (), s32[]{:S(2)}) async-start(), calls=%async_computation.4 | async-start | bytes 2621440 | tf_op jit(solution)/shard_map/reduce_scatter | solution.py:243
  58.5 1.4 copy-start.3
  58.5 4.4 %copy-start.1 = (bf16[8,4,16,2048]{3,2,1,0:T(8,128)(2,1)}, bf16[8,4,16,2048]{3,2,1,0:T(8,128)(2,1)S(1)}, u32[]{:S(2)}) copy-start(bf16[8,4,16,2048]{3,2,1,0:T(8,128)(2,1)S(1)} %get-tuple-element.13) | copy-start | bytes 6291460
  58.6 3.1 %copy-start.4 = (bf16[1,2048,512]{2,1,0:T(8,128)(2,1)S(1)}, bf16[1,2048,512]{2,1,0:T(8,128)(2,1)}, u32[]{:S(2)}) copy-start(bf16[1,2048,512]{2,1,0:T(8,128)(2,1)} %param.22) | copy-start | bytes 6291460
  61.7 1.3 copy-start.10
  61.7 2.0 %copy-start.9 = (bf16[1,512,2048]{2,1,0:T(8,128)(2,1)S(1)}, bf16[1,512,2048]{2,1,0:T(8,128)(2,1)}, u32[]{:S(2)}) copy-start(bf16[1,512,2048]{2,1,0:T(8,128)(2,1)} %param.23) | copy-start | bytes 6291460
  62.9 2.3 %copy-start.12 = (f32[512,512]{1,0:T(8,128)}, f32[512,512]{1,0:T(8,128)S(1)}, u32[]{:S(2)}) copy-start(f32[512,512]{1,0:T(8,128)S(1)} %fusion.9) | copy-start | bytes 3145732
  65.2 1.3 copy-start.6
  69.4 0.8 copy-start.8
  108.5 19.8 %all-to-all-start = ((bf16[8,64,512]{2,1,0:T(8,128)(2,1)}), bf16[8,64,512]{2,1,0:T(8,128)(2,1)S(1)}, u32[]{:S(2)}, u32[]{:S(2)}) async-start(bf16[8,64,512]{2,1,0:T(8,128)(2,1)} %bitcast.114), calls=%async_computation.1 | async-start | bytes 1048576 | tf_op jit(solution)/shard_map/all_to_all | solution.py:244
  114.4 4.5 %copy-start.2 = (bf16[8,4,16,2048]{3,2,1,0:T(8,128)(2,1)S(1)}, bf16[8,4,16,2048]{3,2,1,0:T(8,128)(2,1)}, u32[]{:S(2)}) copy-start(bf16[8,4,16,2048]{3,2,1,0:T(8,128)(2,1)} %copy-done.1) | copy-start | bytes 6291460
  114.4 4.5 %copy-start.11 = (f32[512,512]{1,0:T(8,128)S(1)}, f32[512,512]{1,0:T(8,128)}, u32[]{:S(2)}) copy-start(f32[512,512]{1,0:T(8,128)} %copy-done.10) | copy-start | bytes 3145732
  114.4 4.5 %copy-start.13 = (f32[512,512]{1,0:T(8,128)S(1)}, f32[512,512]{1,0:T(8,128)}, u32[]{:S(2)}) copy-start(f32[512,512]{1,0:T(8,128)} %copy-done.12) | copy-start | bytes 3145732
  121.5 18.4 %copy-start.7 = (bf16[128,512]{1,0:T(8,128)(2,1)S(1)}, bf16[128,512]{1,0:T(8,128)(2,1)}, u32[]{:S(2)}) copy-start(bf16[128,512]{1,0:T(8,128)(2,1)} %param.16) | copy-start | bytes 393220
  136.0 23.5 %all-to-all-start.1 = ((bf16[8,128,256]{2,1,0:T(8,128)(2,1)}), bf16[8,128,256]{2,1,0:T(8,128)(2,1)S(1)}, u32[]{:S(2)}, u32[]{:S(2)}) async-start(bf16[8,128,256]{2,1,0:T(8,128)(2,1)} %bitcast.100), calls=%async_computation.2 | async-start | bytes 1048576 | tf_op jit(solution)/shard_map/all_to_all | solution.py:266
  150.6 6.2 %collective-permute-start = (f32[30,512]{1,0:T(8,128)S(1)}, f32[30,512]{1,0:T(8,128)S(1)}, u32[]{:S(2)}, u32[]{:S(2)}) collective-permute-start(f32[30,512]{1,0:T(8,128)S(1)} %slice.257), channel_id=1, source_target_pairs={{4,0},{8,4},{12,8},{16,12},{20,16},{24,20},{28,24},{5,1},{9,5},{13... | collective-permute-start | bytes 184328 | tf_op jit(solution)/shard_map/ppermute | solution.py:14
Sparse Core Ops, SparseCore 0:
  13.7 50.6 all-gather.1
  69.5 38.9 reduce-scatter.1

commit v3 on v2

--- a/solution.py
+++ b/solution.py
@@ -161,6 +161,126 @@
             flops=0, bytes_accessed=40 * full.size, transcendentals=0
         ),
     )(rows, grads)
+
+
+def home_kernel(experts, groups, partial, home, pair_in, row_out, row_in, total, *sems):
+    pair_send, pair_recv, row_send, row_recv, far_send, far_recv = sems
+    mine = lax.axis_index("sp")
+    place = lax.axis_index("tp")
+    chips = groups // 2
+    chip, core = place // 2, place % 2
+    sibling = chip * 2 + 1 - core
+
+    def at_chip(step):
+        return ((chip + step) % chips) * 2 + core
+
+    barrier = pltpu.get_barrier_semaphore()
+
+    def greet(step, carry):
+        pl.semaphore_signal(barrier, inc=1, device_id=((mine + step) % experts, place),
+                            device_id_type=pl.DeviceIdType.MESH)
+        return carry
+
+    lax.fori_loop(1, experts, greet, 0)
+    for step in range(1, chips):
+        pl.semaphore_signal(barrier, inc=1, device_id=(mine, at_chip(step)),
+                            device_id_type=pl.DeviceIdType.MESH)
+    pl.semaphore_signal(barrier, inc=1, device_id=(mine, sibling),
+                        device_id_type=pl.DeviceIdType.MESH)
+    pl.semaphore_wait(barrier, experts - 1 + chips)
+
+    def pair(step, hop):
+        owner = (mine + step + 1) % experts
+        other = ((chip + hop) % chips) * 2 + 1 - core
+        return remote(partial.at[other, owner], pair_in.at[hop, owner],
+                      pair_send.at[step, hop], pair_recv.at[step, hop], (mine, sibling))
+
+    def row(step, hop):
+        owner = (mine + step + 1) % experts
+        return remote(row_out.at[hop, owner], row_in.at[hop, owner],
+                      row_send.at[step, hop], row_recv.at[step, hop], (mine, at_chip(hop)))
+
+    def far(step):
+        owner = (mine + step + 1) % experts
+        return remote(total.at[owner], home.at[mine],
+                      far_send.at[step], far_recv.at[step], (owner, place))
+
+    def start_pair(step, carry):
+        for hop in reversed(range(chips)):
+            pair(step, hop).start()
+        return carry
+
+    lax.fori_loop(0, experts, start_pair, 0)
+
+    def add_pair(step, hop):
+        owner = (mine + step + 1) % experts
+        pair(step, hop).wait_recv()
+        return partial[at_chip(hop), owner].astype(jnp.float32) + pair_in[hop, owner].astype(
+            jnp.float32
+        )
+
+    def send_rows(step):
+        owner = (mine + step + 1) % experts
+        for hop in range(1, chips):
+            row_out[hop, owner] = add_pair(step, hop).astype(row_out.dtype)
+            row(step, hop).start()
+
+    def add_rows(step):
+        owner = (mine + step + 1) % experts
+        value = add_pair(step, 0)
+        for hop in range(1, chips):
+            row(step, hop).wait_recv()
+            value = value + row_in[hop, owner].astype(jnp.float32)
+        return value.astype(total.dtype)
+
+    def advance(step, carry):
+        send_rows(step)
+        before = step - 1
+        total[(mine + before + 1) % experts] = add_rows(before)
+        far(before).start()
+        return carry
+
+    send_rows(0)
+    lax.fori_loop(1, experts, advance, 0)
+    home[mine] = add_rows(experts - 1)
+
+    def finish(step, carry):
+        for hop in range(chips):
+            pair(step, hop).wait_send()
+            if hop:
+                row(step, hop).wait_send()
+        return carry
+
+    lax.fori_loop(0, experts, finish, 0)
+
+    def finish_far(step, carry):
+        far(step).wait()
+        return carry
+
+    lax.fori_loop(0, experts - 1, finish_far, 0)
+
+
+def home_blocks(partial):
+    groups, experts, capacity, share = partial.shape
+    chips = groups // 2
+    dma = pltpu.SemaphoreType.DMA
+    blocks = pltpu.VMEM((chips, experts, capacity, share), partial.dtype)
+    return pl.pallas_call(
+        functools.partial(home_kernel, experts, groups),
+        out_shape=jax.ShapeDtypeStruct((experts, capacity, share), partial.dtype),
+        in_specs=[pl.BlockSpec(memory_space=pltpu.VMEM)],
+        out_specs=pl.BlockSpec(memory_space=pltpu.VMEM),
+        scratch_shapes=[blocks] * 3
+        + [pltpu.VMEM((experts, capacity, share), partial.dtype)]
+        + [dma((experts, chips))] * 4
+        + [dma((experts,))] * 2,
+        compiler_params=pltpu.CompilerParams(
+            collective_id=1, has_side_effects=True, vmem_limit_bytes=24 * 2**20
+        ),
+        cost_estimate=pl.CostEstimate(
+            flops=0, bytes_accessed=40 * partial.size, transcendentals=0
+        ),
+    )(partial)
 
 
 def shards(
@@ -240,14 +360,7 @@
         partial_value.astype(jnp.bfloat16).reshape(-1, groups, share), (1, 0, 2)
     )
     every_act, partial_groups = lax.optimization_barrier((every_act, partial_groups))
-    summed = lax.psum_scatter(partial_groups, "tp", scatter_dimension=0, tiled=False)
-    home_rows = lax.all_to_all(
-        summed.reshape(experts, capacity, share),
-        "sp",
-        split_axis=0,
-        concat_axis=0,
-        tiled=True,
-    )
+    home_rows = home_blocks(partial_groups.reshape(groups, experts, capacity, share))
     returned = lax.dot_general(
         full_table,
         home_rows.reshape(-1, share),

time: 170 us -> 156 us (0.918)
  waiting for transfers between devices: 44.2 us -> 3.84 us
  Pallas kernels: 43.7 us -> 74.8 us
  starting transfers between devices: 10.9 us -> 7 us
    reduce_scatter x1 -> x0, waiting for transfers between devices: 33.5 us -> none  [shards(): lax.psum_scatter(partial_groups, 'tp', scatter_dimension=0, tiled=False)]
    pallas_call x0 -> x1, Pallas kernels: none -> 31.1 us  [home_blocks(): pl.pallas_call(functools.partial(home_kernel, experts, groups), out_shape...]
    all_to_all x1 -> x0, waiting for transfers between devices: 6.83 us -> none  [shards(): lax.all_to_all(summed.reshape(experts, capacity, share), 'sp', split_axis...]
    all_to_all x1 -> x0, starting transfers between devices: 5.52 us -> none  [shards(): lax.all_to_all(summed.reshape(experts, capacity, share), 'sp', split_axis...]
    dot_general x1, matrix products: 4.43 us -> 2.63 us  [shards(): lax.dot_general(routed_rows, grad_upre, contract_first, preferred_element...]
    unnamed x29 -> x35, local copies, waits for them, and re-layouts: 4.34 us -> 5.16 us
  transfers between devices with their start and end apart: 5 -> 3, of which waited for: 3 -> 1; matrix products, arithmetic and copies ran while one was open for 17% -> 18% of each run, Pallas kernels for 26% -> 28%
where the time goes in v3:
time: 156 us; the launch traced here: 155 us
  Pallas kernels  74.8 us (48%)
  matrix products  23.8 us (15%)
  between operations  14.3 us (9%)
  blocking collectives  13.4 us (9%)
  local copies, waits for them, and re-layouts  10.1 us (6%)
  other arithmetic  7.78 us (5%)
  starting transfers between devices  7 us (4%)
  waiting for transfers between devices  3.84 us (2%)
    pallas_call x1, Pallas kernels, dispatch_blocks(): pl.pallas_call(functools.partial(dispatch_kernel, experts, groups), out_s...  43.7 us
    pallas_call x1, Pallas kernels, home_blocks(): pl.pallas_call(functools.partial(home_kernel, experts, groups), out_shape...  31.1 us
    psum x1, blocking collectives, shards(): lax.psum((jnp.sum(norm_output_gradient, axis=1), jnp.sum(norm_output_grad...  6.92 us
    all_gather x1, blocking collectives, shards(): mixer_grad = lax.all_gather(mixer_share, 'tp', axis=1, tiled=True)  6.5 us
    all_to_all x1, starting transfers between devices, shards(): lax.all_to_all(sent_columns, 'sp', split_axis=0, concat_axis=0, tiled=True)  5.67 us
    unnamed x35, local copies, waits for them, and re-layouts  5.16 us
    dot_general x1, matrix products, shards(): lax.dot_general(routed_rows, grad_gpre, contract_first, preferred_element...  4.35 us
    ppermute x1, waiting for transfers between devices, from_behind(): lax.ppermute(value, axis, [(source, source + steps) for source in range(l...  3.82 us
  transfers between devices with their start and end apart: 3, of which 1 were waited for; matrix products, arithmetic and copies ran while one was open for 18% of the time, Pallas kernels for 28%

profile of v3, /device:TPU:0, one launch (start us, length us, event | category | flops | bytes accessed | tf_op | source)
XLA Modules:
  0.0 155.1 jit_solution(12212289907834196503)
XLA Ops:
  7.2 1.0 copy.36
  8.5 0.6 reduce-window.6
  9.6 0.7 multiply_add_fusion
  10.6 1.3 convolution_convert_fusion.3
  12.0 1.6 %fusion.23 = bf16[128,512]{1,0:T(8,128)(2,1)} fusion(bf16[128,512]{1,0:T(8,128)(2,1)} %param.16, f32[512]{0:T(512)} %param.18), kind=kLoop, calls=%fused_computation.99 | loop fusion | flops 458752 | bytes 264192 | tf_op jit(solution)/shard_map/convert_element_type | solution.py:320
  13.6 0.9 fusion.119
  14.8 43.7 %shard_map.155 = (bf16[8,4,16,2048]{3,2,1,0:T(8,128)(2,1)S(1)}, bf16[8,4,16,2048]{3,2,1,0:T(8,128)(2,1)S(1)}) custom-call(bf16[8,16,2048]{2,1,0:T(8,128)(2,1)S(1)} %bitcast.103, bf16[8,16,2048]{2,1,0:T(8,128)(2,1)S(1)} %bitcast.104), custom_call_target="tpu_custom_call" | custom-call | bytes 41943040 | tf_op jit(solution)/shard_map/pallas_call | solution.py:149
  58.5 1.2 fusion.6
  59.8 1.8 %copy-done.6 = bf16[1,2048,512]{2,1,0:T(8,128)(2,1)S(1)} copy-done((bf16[1,2048,512]{2,1,0:T(8,128)(2,1)S(1)}, bf16[1,2048,512]{2,1,0:T(8,128)(2,1)}, u32[]{:S(2)}) %copy-start.6) | copy-done | bytes 2097176
  61.6 1.2 fusion.9
  62.9 0.7 copy-done.12
  63.6 1.6 %multiply_convert_fusion.1 = (bf16[512,512]{1,0:T(8,128)(2,1)S(1)}, bf16[512,512]{1,0:T(8,128)(2,1)S(1)}) fusion(f32[512,512]{1,0:T(8,128)S(1)} %fusion.6, f32[512,512]{1,0:T(8,128)S(1)} %fusion.9, bf16[512,2048]{1,0:T(8,128)(2,1)S(1)} %bitcast.105, bf16[1,512,2048]{2,1,0:T(8,128)(2,1)S(1)} %copy-done.12), kind=kOutput, calls=%fused_computation.55 | convolution fusion | flops 1077149696 | bytes 7340032 | tf_op jit(solution)/shard_map/dot_general | solution.py:342
  65.2 1.3 fusion.4
  66.5 1.3 add_convert_fusion
  67.8 1.5 copy.45
  69.7 0.7 fusion.125
  70.3 4.4 %fusion = bf16[1,2048,512]{2,1,0:T(8,128)(2,1)} fusion(bf16[512,2048]{1,0:T(8,128)(2,1)} %bitcast.109, bf16[512,512]{1,0:T(8,128)(2,1)S(1)} %get-tuple-element.22), kind=kOutput, calls=%fused_computation.33 | convolution fusion | flops 1074790400 | bytes 4718592 | tf_op jit(solution)/shard_map/dot_general | solution.py:349
  74.7 2.6 %fusion.1 = bf16[1,2048,512]{2,1,0:T(8,128)(2,1)} fusion(bf16[512,2048]{1,0:T(8,128)(2,1)S(1)} %bitcast.110, bf16[512,512]{1,0:T(8,128)(2,1)S(1)} %copy-done.9), kind=kOutput, calls=%fused_computation.34 | convolution fusion | flops 1074790400 | bytes 4718592 | tf_op jit(solution)/shard_map/dot_general | solution.py:352
  77.3 2.7 %fusion.2 = bf16[1,512,2048]{2,1,0:T(8,128)(2,1)} fusion(bf16[512,2048]{1,0:T(8,128)(2,1)S(1)} %bitcast.106, f32[512,512]{1,0:T(8,128)S(1)} %copy-done.16, f32[512,512]{1,0:T(8,128)S(1)} %copy-done.14), kind=kOutput, calls=%fused_computation.35 | convolution fusion | flops 1076363264 | bytes 6291456 | tf_op jit(solution)/shard_map/dot_general | solution.py:339
  80.1 1.6 %copy-done.1 = bf16[64,4,8,512]{3,2,0,1:T(8,128)(2,1)S(1)} copy-done((bf16[64,4,8,512]{3,2,0,1:T(8,128)(2,1)S(1)}, bf16[64,4,8,512]{3,2,0,1:T(8,128)(2,1)}, u32[]{:S(2)}) %copy-start.1) | copy-done | bytes 2097176
  81.6 31.1 %shard_map.156 = bf16[8,64,512]{2,1,0:T(8,128)(2,1)S(1)} custom-call(bf16[4,8,64,512]{3,2,1,0:T(8,128)(2,1)S(1)} %bitcast.101), custom_call_target="tpu_custom_call" | custom-call | bytes 41943040 | tf_op jit(solution)/shard_map/pallas_call | solution.py:268
  113.1 6.5 %all_gather.7 = bf16[128,2048]{1,0:T(8,128)(2,1)S(1)} all-gather(bf16[128,512]{1,0:T(8,128)(2,1)S(1)} %fusion.15), channel_id=1, replica_groups=mesh['sp'=8,'tp'=4] {'tp'}, dimensions={1}, use_global_device_ids=true | all-gather | bytes 655360 | tf_op jit(solution)/shard_map/all_gather | solution.py:374
  119.6 0.8 copy.46
  120.4 5.7 %all-to-all-start = ((bf16[8,128,256]{2,1,0:T(8,128)(2,1)}), bf16[8,128,256]{2,1,0:T(8,128)(2,1)S(1)}, u32[]{:S(2)}, u32[]{:S(2)}) async-start(bf16[8,128,256]{2,1,0:T(8,128)(2,1)} %bitcast.100), calls=%async_computation | async-start | bytes 1048576 | tf_op jit(solution)/shard_map/all_to_all | solution.py:379
  126.1 3.1 %fusion.124 = (f32[128]{0:T(128)}, f32[128]{0:T(128)}, f32[128,512]{1,0:T(8,128)S(1)}) fusion(bf16[128,512]{1,0:T(8,128)(2,1)S(1)} %copy-done.10, f32[512]{0:T(512)} %param.18, bf16[128,2048]{1,0:T(8,128)(2,1)S(1)} %all_gather.7, bf16[512,2048]{1,0:T(8,128)(2,1)} %param.20), kind=kOutput, calls=%fused_computation.213 | convolution fusion | flops 269352704 | bytes 3017728 | tf_op jit(solution)/shard_map/dot_general | solution.py:385
  129.2 6.9 %all-reduce = (f32[128]{0:T(128)S(1)}, f32[128]{0:T(128)S(1)}) all-reduce(f32[128]{0:T(128)} %get-tuple-element.18, f32[128]{0:T(128)} %get-tuple-element.17), channel_id=1, replica_groups=mesh['sp'=8,'tp'=4] {'tp'}, use_global_device_ids=true, to_apply=%region_9.10 | all-reduce | flops 256 | bytes 2048 | tf_op jit(solution)/shard_map/psum | solution.py:394
  136.1 0.8 fusion.27
  136.9 1.3 collective-permute-start
  138.2 1.0 fusion.126
  139.3 3.8 %collective-permute-done = f32[30,512]{1,0:T(8,128)S(1)} collective-permute-done((f32[30,512]{1,0:T(8,128)S(1)}, f32[30,512]{1,0:T(8,128)S(1)}, u32[]{:S(2)}, u32[]{:S(2)}) %collective-permute-start) | collective-permute-done | bytes 61472 | tf_op jit(solution)/shard_map/ppermute | solution.py:14
  143.1 2.7 %fusion.32 = bf16[128,512]{1,0:T(8,128)(2,1)} fusion(f32[128,512]{1,0:T(8,128)S(1)} %fusion.27, f32[30,512]{1,0:T(8,128)S(1)} %collective-permute-done, f32[512]{0:T(512)S(1)} %bitcast.143, f32[512]{0:T(512)S(1)} %bitcast.144, f32[512]{0:T(512)S(1)} %bitcast.115, f32[512]{0:T(512)S(1)} %bitcast.116, f32[512]{0:T(512)S(1)} %bitcast.117, f32[512]{0:T(512)} %bitcast.118, ...), kind=kLoop, calls=%fused_computation.108 | loop fusion | flops 6029312 | bytes 518144 | tf_op jit(solution)/shard_map/convert_element_type | solution.py:414
  145.8 2.5 %fusion.127 = f32[256,512]{1,0:T(8,128)} fusion(bf16[1024,256]{1,0:T(8,128)(2,1)S(1)} %bitcast.113, bf16[1024,512]{1,0:T(8,128)(2,1)} %all-gather.2.cloned.1.call-done), kind=kOutput, calls=%fused_computation.216 | convolution fusion | flops 268435456 | bytes 2097152 | tf_op jit(solution)/shard_map/dot_general | solution.py:382
  (56 shorter events, 2.1 us)
Async XLA Ops:
  7.2 51.3 %copy-start = (bf16[1,2048,512]{2,1,0:T(8,128)(2,1)S(1)}, bf16[1,2048,512]{2,1,0:T(8,128)(2,1)}, u32[]{:S(2)}) copy-start(bf16[1,2048,512]{2,1,0:T(8,128)(2,1)} %param.21) | copy-start | bytes 6291460
  7.2 7.3 %copy-start.7 = (bf16[128,2048]{1,0:T(8,128)(2,1)S(1)}, bf16[128,2048]{1,0:T(8,128)(2,1)}, u32[]{:S(2)}) copy-start(bf16[128,2048]{1,0:T(8,128)(2,1)} %param.12) | copy-start | bytes 1572868
  7.2 72.9 %all-gather.2.cloned.1.call-start = ((), (), s32[]{:S(2)}) async-start(), calls=%async_computation.1 | async-start | bytes 1179648 | tf_op jit(solution)/shard_map/all_gather | solution.py:322
  58.5 1.3 copy-start.4
  58.5 4.4 %copy-start.2 = (bf16[8,4,16,2048]{3,2,1,0:T(8,128)(2,1)}, bf16[8,4,16,2048]{3,2,1,0:T(8,128)(2,1)S(1)}, u32[]{:S(2)}) copy-start(bf16[8,4,16,2048]{3,2,1,0:T(8,128)(2,1)S(1)} %get-tuple-element.13) | copy-start | bytes 6291460
  58.5 3.1 %copy-start.6 = (bf16[1,2048,512]{2,1,0:T(8,128)(2,1)S(1)}, bf16[1,2048,512]{2,1,0:T(8,128)(2,1)}, u32[]{:S(2)}) copy-start(bf16[1,2048,512]{2,1,0:T(8,128)(2,1)} %param.22) | copy-start | bytes 6291460
  61.6 1.3 copy-start.13
  61.6 2.0 %copy-start.12 = (bf16[1,512,2048]{2,1,0:T(8,128)(2,1)S(1)}, bf16[1,512,2048]{2,1,0:T(8,128)(2,1)}, u32[]{:S(2)}) copy-start(bf16[1,512,2048]{2,1,0:T(8,128)(2,1)} %param.23) | copy-start | bytes 6291460
  62.9 2.3 %copy-start.15 = (f32[512,512]{1,0:T(8,128)}, f32[512,512]{1,0:T(8,128)S(1)}, u32[]{:S(2)}) copy-start(f32[512,512]{1,0:T(8,128)S(1)} %fusion.9) | copy-start | bytes 3145732
  65.2 1.3 copy-start.8
  67.8 1.9 %copy-start.11 = (f32[31,512]{1,0:T(8,128)S(1)}, f32[31,512]{1,0:T(8,128)}, u32[]{:S(2)}) copy-start(f32[31,512]{1,0:T(8,128)} %param.19) | copy-start | bytes 190468
  70.3 4.4 %copy-start.5 = (bf16[8,4,16,2048]{3,2,1,0:T(8,128)(2,1)S(1)}, bf16[8,4,16,2048]{3,2,1,0:T(8,128)(2,1)}, u32[]{:S(2)}) copy-start(bf16[8,4,16,2048]{3,2,1,0:T(8,128)(2,1)} %copy-done.4) | copy-start | bytes 6291460
  70.3 4.4 %copy-start.9 = (bf16[512,512]{1,0:T(8,128)(2,1)S(1)}, bf16[512,512]{1,0:T(8,128)(2,1)}, u32[]{:S(2)}) copy-start(bf16[512,512]{1,0:T(8,128)(2,1)} %copy-done.8) | copy-start | bytes 1572868
  74.7 2.6 %copy-start.3 = (bf16[8,4,16,2048]{3,2,1,0:T(8,128)(2,1)S(1)}, bf16[8,4,16,2048]{3,2,1,0:T(8,128)(2,1)}, u32[]{:S(2)}) copy-start(bf16[8,4,16,2048]{3,2,1,0:T(8,128)(2,1)} %copy-done.2) | copy-start | bytes 6291460
  74.7 2.6 %copy-start.14 = (f32[512,512]{1,0:T(8,128)S(1)}, f32[512,512]{1,0:T(8,128)}, u32[]{:S(2)}) copy-start(f32[512,512]{1,0:T(8,128)} %copy-done.13) | copy-start | bytes 3145732
  74.7 2.6 %copy-start.16 = (f32[512,512]{1,0:T(8,128)S(1)}, f32[512,512]{1,0:T(8,128)}, u32[]{:S(2)}) copy-start(f32[512,512]{1,0:T(8,128)} %copy-done.15) | copy-start | bytes 3145732
  80.1 1.6 %copy-start.1 = (bf16[64,4,8,512]{3,2,0,1:T(8,128)(2,1)S(1)}, bf16[64,4,8,512]{3,2,0,1:T(8,128)(2,1)}, u32[]{:S(2)}) copy-start(bf16[64,4,8,512]{3,2,0,1:T(8,128)(2,1)} %copy.45) | copy-start | bytes 6291460
  112.8 13.3 %copy-start.10 = (bf16[128,512]{1,0:T(8,128)(2,1)S(1)}, bf16[128,512]{1,0:T(8,128)(2,1)}, u32[]{:S(2)}) copy-start(bf16[128,512]{1,0:T(8,128)(2,1)} %param.16) | copy-start | bytes 393220
  120.4 25.4 %all-to-all-start = ((bf16[8,128,256]{2,1,0:T(8,128)(2,1)}), bf16[8,128,256]{2,1,0:T(8,128)(2,1)S(1)}, u32[]{:S(2)}, u32[]{:S(2)}) async-start(bf16[8,128,256]{2,1,0:T(8,128)(2,1)} %bitcast.100), calls=%async_computation | async-start | bytes 1048576 | tf_op jit(solution)/shard_map/all_to_all | solution.py:379
  136.9 6.2 %collective-permute-start = (f32[30,512]{1,0:T(8,128)S(1)}, f32[30,512]{1,0:T(8,128)S(1)}, u32[]{:S(2)}, u32[]{:S(2)}) collective-permute-start(f32[30,512]{1,0:T(8,128)S(1)} %slice.257), channel_id=1, source_target_pairs={{4,0},{8,4},{12,8},{16,12},{20,16},{24,20},{28,24},{5,1},{9,5},{13... | collective-permute-start | bytes 184328 | tf_op jit(solution)/shard_map/ppermute | solution.py:14
Sparse Core Ops, SparseCore 0:
  13.7 50.6 all-gather.1
